TPU v7x, 256 devices: a whole 4x4x8 slice. The times are simulated.
256 devices in a mesh: sp: 64 (over z, x, core), tp: 4 (over y).
Axes of the slice: x: 4, y: 4, z: 8, core: 2. Of those that a mesh axis runs over, the one named last changes fastest.
Arguments:
- residual: bfloat16 [16384, 2048], P(('sp', 'tp')), may hold values from -6 to 6
- queries: bfloat16 [16384, 512], P('sp', 'tp'), may hold values from -6 to 6
- projected_keys: bfloat16 [16384, 512], P('sp', 'tp'), may hold values from -6 to 6
- values: bfloat16 [16384, 1024], P('sp', 'tp'), may hold values from -6 to 6
- projected_output_gate: bfloat16 [16384, 1024], P('sp', 'tp'), may hold values from -6 to 6
- decay_gate_input: bfloat16 [16384, 512], P('sp', 'tp'), may hold values from -7 to 7
- decay_gate_offset: float32 [512], P('tp')
- decay_spikes: float32 [16384, 16], P('sp', 'tp'), may hold values from -3 to 0, as said below
- documents: int32 [16384], P('sp'), may hold values from 0 to 31, as said below
- attention_output_weight: bfloat16 [1024, 2048], P('tp'), may hold values from -0.1875 to 0.1875
- layer_norm_gains: float32 [2, 2048], replicated, may hold values from 0.1 to 1.9
- layer_norm_shifts: float32 [2, 2048], replicated, may hold values from -3 to 3
- routes: int32 [16384, 2], P('sp'), may hold values from 0 to 63, all different within a row; in each aligned block of 64 rows (0 to 63, 64 to 127, ...) at most 4 rows name the same one
- chosen_expert_weights: float32 [16384, 2], P('sp'), may hold values from 0.2 to 1
- expert_gate_weight: bfloat16 [64, 2048, 3584], P('sp', None, 'tp'), may hold values from -0.125 to 0.125
- expert_up_weight: bfloat16 [64, 2048, 3584], P('sp', None, 'tp'), may hold values from -0.125 to 0.125
- expert_down_weight: bfloat16 [64, 3584, 2048], P('sp', 'tp'), may hold values from -0.09375 to 0.09375
Outputs:
- layer_out: bfloat16 [16384, 2048], P(('sp', 'tp'))
Inputs may be any that keep to these rules, and one draw needn't show every extreme that they name: `routes`: each row names 2 different experts; in each aligned block of 64 rows no expert is named by more than 4 rows. `documents`: the first position has document 0; document numbers never fall and rise by at most one from a position to the next. `decay_spikes`: zero at all but a few positions.
All inputs are finite; a program needn't handle non-finite values.
Results may differ from a plain program's by a relative error of at most 0.015.
Values may be sent and summed in bfloat16 or wider, within the bound.
A program may use at most 64 MiB of HBM per device.

v0:
```python
import jax
import jax.numpy as jnp
from jax import lax
from jax.sharding import Mesh
from jax.sharding import PartitionSpec as P

BLOCK = 64
SP = ("sp_0", "sp_1", "sp_2")
SP_TP = ("sp_0", "sp_1", "sp_2", "tp")


eps_rms = 1e-06
eps_layer = 1e-05
decay_norm = 16.0


def nothing_yet(array, identity):
    return jax.tree.map(
        lambda a, e: jnp.broadcast_to(jnp.asarray(e, a.dtype), a.shape), array, identity
    )


def gathered_once(array, axis):
    leaves = jax.tree.leaves(array)
    turns = sorted(range(len(leaves)), key=lambda k: -leaves[k].size)
    width = (1, *leaves[turns[0]].shape)[-1]
    lines = [
        jnp.pad(leaves[k].reshape(-1), (0, -leaves[k].size % width)).reshape(-1, width)
        for k in turns
    ]
    both, at, found = (lax.all_gather(jnp.concatenate(lines), axis), 0, {})
    for k, line in zip(turns, lines):
        section = both[:, at : at + len(line)].reshape(len(both), -1)
        found[k] = section[:, : leaves[k].size].reshape(-1, *leaves[k].shape)
        at += len(line)
    numbers = iter(range(len(leaves)))
    return jax.tree.map(lambda _: found[next(numbers)], array)


def entering(array, axes, combine, identity):
    before = start = nothing_yet(array, identity)
    running = array
    for axis in reversed(axes):
        peers, here = (lax.axis_size(axis), lax.axis_index(axis))
        pieces = gathered_once(
            jax.tree.map(
                lambda part, kind: part.astype(kind),
                running,
                (jnp.bfloat16, jnp.bfloat16, jnp.bfloat16, jnp.bfloat16),
            ),
            axis,
        )
        inside, running = (start, start)
        for k in range(peers):
            passed = k < here
            running = combine(
                running, jax.tree.map(lambda part, own: part[k].astype(own.dtype), pieces, array)
            )
            inside = jax.tree.map(lambda new, old: jnp.where(passed, new, old), running, inside)
        before = combine(inside, before)
    return before


def cut_along(array, dim, peers):
    shape = array.shape
    pieces = array.reshape(*shape[:dim], peers, shape[dim] // peers, *shape[dim + 1 :])
    return jnp.moveaxis(pieces, dim, 0)


def summed_on_arrival(array, axis, dim):
    peers = lax.axis_size(axis)
    pieces = lax.all_to_all(cut_along(array, dim, peers), axis, 0, 0, tiled=True)
    return jnp.sum(pieces.astype(jnp.float32), axis=0)


def log_decay_values(decay_gate_input, decay_gate_offset, decay_spikes):
    head_number = decay_spikes.shape[1]
    log_rate_values = (
        jax.nn.log_sigmoid(decay_gate_input.astype(jnp.float32) + decay_gate_offset) / decay_norm
    )
    return (
        log_rate_values.reshape(log_rate_values.shape[0], head_number, -1)
        + decay_spikes[:, :, None]
    )


def block_pass(carry_in, block_inputs):
    current_state, state_doc = carry_in
    query_block, key_blk, value_block, rate_blk, doc_blk = block_inputs
    sequence_length = doc_blk.shape[0]
    running_total = jnp.cumsum(rate_blk, axis=0)
    row_ids = lax.broadcasted_iota(jnp.int32, (sequence_length, sequence_length), 0)
    col_ids = lax.broadcasted_iota(jnp.int32, (sequence_length, sequence_length), 1)
    visible = (row_ids >= col_ids) & (doc_blk[:, None] == doc_blk[None, :])
    spread = running_total[:, None] - running_total[None, :]
    decay_pairs = jnp.exp(jnp.where(visible[:, :, None, None], spread, -jnp.inf))
    scores = jnp.sum(query_block[:, None] * decay_pairs * key_blk[None, :], axis=-1)
    inner_term = jnp.einsum("tsh,shv->thv", scores, value_block)
    active_mask = (doc_blk == state_doc).astype(jnp.float32)
    carried_over = (
        jnp.einsum("nws,wse->nwe", query_block * jnp.exp(running_total), current_state)
        * active_mask[:, None, None]
    )
    last_doc = doc_blk[sequence_length - 1].astype(jnp.float32)
    tail_mask = (doc_blk == last_doc).astype(jnp.float32)
    document_key_ends = (
        key_blk
        * jnp.exp(running_total[sequence_length - 1][None] - running_total)
        * tail_mask[:, None, None]
    )
    keep_state = (state_doc == last_doc).astype(jnp.float32)
    updated_state = (
        current_state * (jnp.exp(running_total[sequence_length - 1]) * keep_state)[:, :, None]
    )
    updated_state = updated_state + jnp.einsum("elr,elo->lro", document_key_ends, value_block)
    return ((updated_state, last_doc), inner_term + carried_over)


def layer_norm(stream, gain_row, shift_row):
    center = jnp.mean(stream, axis=-1, keepdims=True)
    spread = jnp.mean(jnp.square(stream - center), axis=-1, keepdims=True)
    return (stream - center) * lax.rsqrt(spread + eps_layer) * gain_row + shift_row


def link_states(earlier, later):
    first_a, last_a, decay_a, state_a = earlier
    first_b, last_b, decay_b, state_b = later
    joined = (first_b == last_b) & ((last_a == first_b) | (last_a < 0) | (first_b < 0))
    first_doc = jnp.where(first_a >= 0, first_a, first_b)
    last_doc = jnp.where(last_b >= 0, last_b, last_a)
    decay_now = jnp.where(joined, decay_a * decay_b, decay_b)
    current_state = jnp.where(joined, state_a * decay_b[..., None] + state_b, state_b)
    return (first_doc, last_doc, decay_now, current_state)


def slot_index(route_rows, block_rows, capacity, expert_count):
    row_total, top_count = route_rows.shape
    sources = row_total // block_rows
    flat_routes = route_rows.reshape(sources, block_rows * top_count)
    expert_marks = (
        flat_routes[:, :, None] == lax.broadcasted_iota(jnp.int32, (1, 1, expert_count), 2)
    ).astype(jnp.int32)
    before = jnp.cumsum(expert_marks, axis=1) - expert_marks
    position = jnp.sum(before * expert_marks, axis=2)
    source_id = lax.broadcasted_iota(jnp.int32, position.shape, 0)
    slots = flat_routes * (sources * capacity) + source_id * capacity + position
    return slots.reshape(row_total, top_count)


def fill_slots(row_block, slots, slot_total):
    owners = lax.broadcasted_iota(jnp.int32, slots.shape, 0).reshape(-1)
    slot_owner = (
        jnp.full((slot_total,), slots.shape[0], jnp.int32).at[slots.reshape(-1)].set(owners)
    )
    return jnp.take(row_block, slot_owner, axis=0, mode="fill", fill_value=0)


def expert_quarter(row_block, gate_part, up_part, down_part):
    gate_val = jnp.dot(row_block, gate_part, preferred_element_type=jnp.float32)
    up_val = jnp.dot(row_block, up_part, preferred_element_type=jnp.float32)
    hidden = (jax.nn.silu(gate_val) * up_val).astype(jnp.bfloat16)
    return jnp.dot(hidden, down_part, preferred_element_type=jnp.float32).astype(jnp.bfloat16)


def combine_rows(returned, slots, weight_rows):
    model_width = returned.shape[-1]
    picked = jnp.take(returned.reshape(-1, model_width), slots.reshape(-1), axis=0)
    picked = picked.reshape(slots.shape + (model_width,))
    return jnp.sum(picked * weight_rows[:, :, None], axis=1)


def on_device(
    residual,
    queries,
    projected_keys,
    values,
    projected_output_gate,
    decay_gate_input,
    decay_gate_offset,
    decay_spikes,
    documents,
    attention_output_weight,
    layer_norm_gains,
    layer_norm_shifts,
    routes,
    chosen_expert_weights,
    expert_gate_weight,
    expert_up_weight,
    expert_down_weight,
):
    sequence_length, head_number = decay_spikes.shape
    key_dim = queries.shape[1] // head_number
    value_dim = values.shape[1] // head_number
    rows_dev, model_width = residual.shape
    expert_count = lax.axis_size(SP)
    capacity = max(2, 4 * rows_dev // expert_count)
    query_f = queries.astype(jnp.float32).reshape(
        sequence_length, head_number, key_dim
    ) * key_dim ** (-0.5)
    key_f = projected_keys.astype(jnp.float32).reshape(sequence_length, head_number, key_dim)
    value_float = values.astype(jnp.float32).reshape(sequence_length, head_number, value_dim)
    log_rate_values = log_decay_values(decay_gate_input, decay_gate_offset, decay_spikes)
    running_total = jnp.cumsum(log_rate_values, axis=0)
    block_count = sequence_length // BLOCK

    def blocked(whole_array):
        return whole_array.reshape((block_count, BLOCK) + whole_array.shape[1:])

    block_inputs = (
        blocked(query_f),
        blocked(key_f),
        blocked(value_float),
        blocked(log_rate_values),
        blocked(documents),
    )
    zero_state = jnp.zeros((head_number, key_dim, value_dim), jnp.float32)
    identity = (
        jnp.array(-1.0, jnp.float32),
        jnp.array(-1.0, jnp.float32),
        jnp.ones((head_number, key_dim), jnp.float32),
        zero_state,
    )
    first_doc = documents[0].astype(jnp.float32)
    last_doc = documents[sequence_length - 1].astype(jnp.float32)
    tail_mask = (documents == documents[sequence_length - 1]).astype(jnp.float32)
    document_key_ends = (
        key_f
        * jnp.exp(running_total[sequence_length - 1][None] - running_total)
        * tail_mask[:, None, None]
    )
    shard_local_state = jnp.einsum("elr,elo->lro", document_key_ends, value_float)
    prefix = entering(
        (first_doc, last_doc, jnp.exp(running_total[sequence_length - 1]), shard_local_state),
        SP,
        link_states,
        identity,
    )
    _, block_outputs = lax.scan(block_pass, (prefix[3], prefix[1]), block_inputs)
    recurrent = block_outputs.reshape(sequence_length, head_number, value_dim)
    norm_scale = lax.rsqrt(jnp.mean(recurrent * recurrent, axis=-1, keepdims=True) + eps_rms)
    gate_act = jax.nn.silu(
        projected_output_gate.astype(jnp.float32).reshape(sequence_length, head_number, value_dim)
    )
    mixed = (
        (recurrent * norm_scale * gate_act)
        .reshape(sequence_length, head_number * value_dim)
        .astype(jnp.bfloat16)
    )
    projected = summed_on_arrival(
        jnp.dot(mixed, attention_output_weight, preferred_element_type=jnp.float32).astype(
            jnp.bfloat16
        ),
        "tp",
        0,
    )
    normed = layer_norm(
        residual.astype(jnp.float32) + projected, layer_norm_gains[0], layer_norm_shifts[0]
    ).astype(jnp.bfloat16)
    own_routes = lax.dynamic_slice_in_dim(routes, lax.axis_index("tp") * rows_dev, rows_dev, 0)
    own_weights = lax.dynamic_slice_in_dim(
        chosen_expert_weights, lax.axis_index("tp") * rows_dev, rows_dev, 0
    )
    slots = slot_index(own_routes, rows_dev, capacity, expert_count)
    outgoing = fill_slots(normed, slots, expert_count * capacity).reshape(
        expert_count, capacity, model_width
    )
    all_rows = lax.all_gather(
        lax.all_to_all(outgoing, SP, split_axis=0, concat_axis=0, tiled=True),
        "tp",
        axis=1,
        tiled=True,
    )
    sources, slot_count, _ = all_rows.shape
    partial_value = expert_quarter(
        all_rows.reshape(sources * slot_count, model_width),
        expert_gate_weight[0],
        expert_up_weight[0],
        expert_down_weight[0],
    )
    summed = lax.psum_scatter(
        partial_value.reshape(sources, slot_count, model_width)
        .astype(jnp.float32)
        .astype(jnp.bfloat16),
        "tp",
        scatter_dimension=1,
        tiled=True,
    ).astype(jnp.float32)
    returned = lax.all_to_all(
        summed.astype(jnp.bfloat16), SP, split_axis=0, concat_axis=0, tiled=True
    ).astype(summed.dtype)
    expert_mix = combine_rows(returned, slots, own_weights)
    return layer_norm(
        normed.astype(jnp.float32) + expert_mix, layer_norm_gains[1], layer_norm_shifts[1]
    ).astype(jnp.bfloat16)


def solution(mesh):
    torus = Mesh(mesh.devices.reshape(8, 4, 2, mesh.shape["tp"]), ("sp_0", "sp_1", "sp_2", "tp"))
    return jax.shard_map(
        on_device,
        mesh=torus,
        in_specs=(
            P(SP_TP, None),
            P(SP, "tp"),
            P(SP, "tp"),
            P(SP, "tp"),
            P(SP, "tp"),
            P(SP, "tp"),
            P("tp"),
            P(SP, "tp"),
            P(SP),
            P("tp", None),
            P(),
            P(),
            P(SP, None),
            P(SP, None),
            P(SP, None, "tp"),
            P(SP, None, "tp"),
            P(SP, "tp", None),
        ),
        out_specs=P(SP_TP, None),
        check_vma=False,
    )
```

profile of v0, /device:TPU:1, one launch (start us, length us, event | category | flops | bytes accessed | tf_op | source)
XLA Modules:
  0.0 402.5 jit_solution(17770649913272295131)
XLA Ops:
  6.5 1.5 fusion.75
  8.7 1.4 compare_convert_fusion.2
  12.6 2.3 reduce-window.6
  19.2 4.7 %all-gather.3 = bf16[2,132,64]{1,2,0:T(8,128)(2,1)S(1)} all-gather(bf16[1,132,64]{1,2,0:T(8,128)(2,1)S(1)} %maximum_bitcast_fusion.1), channel_id=2, replica_groups=mesh['sp_0'=8,'sp_1'=4,'sp_2'=2,'tp'=4] {'sp_2'}, dimensions={0}, use_global_device_ids=true | all-gather | bytes 50688 | tf_op jit(solution)/shard_map/all_gather | solution.py:31
  33.6 9.1 %all-gather.4 = bf16[4,132,64]{1,2,0:T(8,128)(2,1)S(1)} all-gather(bf16[1,132,64]{1,2,0:T(8,128)(2,1)S(1)} %maximum_bitcast_fusion.2), channel_id=3, replica_groups=mesh['sp_0'=8,'sp_1'=4,'sp_2'=2,'tp'=4] {'sp_1'}, dimensions={0}, use_global_device_ids=true | all-gather | bytes 84480 | tf_op jit(solution)/shard_map/all_gather | solution.py:31
  67.6 21.0 %all-gather.5 = bf16[8,132,64]{1,2,0:T(8,128)(2,1)S(1)} all-gather(bf16[1,132,64]{1,2,0:T(8,128)(2,1)S(1)} %copy.537), channel_id=4, replica_groups=mesh['sp_0'=8,'sp_1'=4,'sp_2'=2,'tp'=4] {'sp_0'}, dimensions={0}, use_global_device_ids=true | all-gather | bytes 152064 | tf_op jit(solution)/shard_map/all_gather | solution.py:31
  127.3 1.4 broadcast_add_fusion
  130.6 28.0 %while.14 = (s32[]{:T(128)}, f32[4,32,64]{2,1,0:T(8,128)S(1)}, f32[]{:T(128)}, f32[4,64,4,64]{1,3,2,0:T(8,128)S(1)}, f32[4,64,4,32]{1,0,3,2:T(4,128)}, /*index=5...) while((s32[]{:T(128)}, f32[4,32,64]{2,1,0:T(8,128)S(1)}, ...), condition=%wide.region_5.6_spmd, body=%wide.region_2.5_spmd.sunk | while | flops 7426565 | bytes 1488051 | solution.py:238
  134.8 2.6 multiply_reduce_fusion.6
  141.8 2.6 multiply_reduce_fusion.6
  148.8 2.6 multiply_reduce_fusion.6
  155.8 2.6 multiply_reduce_fusion.6
  159.6 1.5 convolution_convert_fusion.1
  161.1 4.2 %all-to-all-start = ((bf16[4,64,2048]{2,1,0:T(8,128)(2,1)}), bf16[4,64,2048]{2,1,0:T(8,128)(2,1)S(1)}, u32[]{:S(2)}, u32[]{:S(2)}) async-start(bf16[4,64,2048]{2,1,0:T(8,128)(2,1)} %bitcast.115), calls=%async_computation | async-start | bytes 2097152 | tf_op jit(solution)/shard_map/all_to_all | solution.py:72
  167.6 7.4 %all-to-all-done = bf16[4,64,2048]{2,1,0:T(8,128)(2,1)S(1)} async-done(((bf16[4,64,2048]{2,1,0:T(8,128)(2,1)}), bf16[4,64,2048]{2,1,0:T(8,128)(2,1)S(1)}, u32[]{:S(2)}, u32[]{:S(2)}) %all-to-all-start) | async-done | bytes 1048608 | tf_op jit(solution)/shard_map/all_to_all | solution.py:72
  175.7 1.4 gather_fusion
  178.1 46.3 %all_to_all.15 = bf16[64,4,2048]{2,1,0:T(4,128)(2,1)S(1)} all-to-all(bf16[64,4,2048]{2,1,0:T(4,128)(2,1)S(1)} %broadcast_select_fusion), channel_id=1, replica_groups=mesh['sp_0'=8,'sp_1'=4,'sp_2'=2,'tp'=4] {'sp_0','sp_1','sp_2'}, dimensions={0} | all-to-all | bytes 2097152 | tf_op jit(solution)/shard_map/all_to_all | solution.py:268
  224.3 1.6 copy.570
  225.9 45.8 %all-gather.8.cloned.1.call-done = bf16[64,16,2048]{2,0,1:T(8,128)(2,1)} async-done(((bf16[64,4,2048]{2,0,1:T(8,128)(2,1)}), bf16[64,16,2048]{2,0,1:T(8,128)(2,1)}) %all-gather.8.cloned.1.call-update) | async-done | bytes 4194320 | tf_op jit(solution)/shard_map/all_gather | solution.py:267
  271.7 4.6 %copy.571 = bf16[64,16,2048]{2,1,0:T(8,128)(2,1)S(1)} copy(bf16[64,16,2048]{2,0,1:T(8,128)(2,1)} %all-gather.8.cloned.1.call-done) | data formatting | bytes 8388608 | tf_op jit(solution)/shard_map/all_gather | solution.py:267
  276.4 4.5 %fusion.11 = f32[1024,896]{1,0:T(8,128)S(1)} fusion(bf16[1024,2048]{1,0:T(8,128)(2,1)S(1)} %bitcast.268, bf16[1,2048,896]{2,1,0:T(8,128)(2,1)S(1)} %copy-done.11), kind=kOutput, calls=%fused_computation.32 | convolution fusion | flops 3758096384 | bytes 11534336 | tf_op jit(solution)/shard_map/dot_general | solution.py:160
  280.9 4.8 %multiply_convert_fusion = bf16[1024,896]{1,0:T(8,128)(2,1)S(1)} fusion(f32[1024,896]{1,0:T(8,128)S(1)} %fusion.11, bf16[1024,2048]{1,0:T(8,128)(2,1)S(1)} %bitcast.269, bf16[1,2048,896]{2,1,0:T(8,128)(2,1)S(1)} %copy-done.12), kind=kOutput, calls=%fused_computation.36 | convolution fusion | flops 3763601408 | bytes 13369344 | tf_op jit(solution)/shard_map/dot_general | solution.py:159
  285.7 4.9 %convolution_convert_fusion = bf16[1024,2048]{1,0:T(8,128)(2,1)S(1)} fusion(bf16[1024,896]{1,0:T(8,128)(2,1)S(1)} %multiply_convert_fusion, bf16[1,896,2048]{2,1,0:T(8,128)(2,1)S(1)} %copy-done.13), kind=kOutput, calls=%fused_computation.30 | convolution fusion | flops 3760193536 | bytes 9699328 | tf_op jit(solution)/shard_map/dot_general | solution.py:162
  290.7 4.2 %copy.572 = bf16[64,16,2048]{2,0,1:T(8,128)(2,1)} copy(bf16[64,16,2048]{2,1,0:T(8,128)(2,1)S(1)} %bitcast.270) | data formatting | bytes 8388608 | tf_op jit(solution)/shard_map/reshape | solution.py:281
  294.9 50.0 %reduce-scatter.2.cloned.1.call-done = bf16[64,4,2048]{2,0,1:T(8,128)(2,1)} async-done(((bf16[64,16,2048]{2,0,1:T(8,128)(2,1)}), bf16[64,4,2048]{2,0,1:T(8,128)(2,1)}) %reduce-scatter.2.cloned.1.call-update) | async-done | bytes 1048592 | tf_op jit(solution)/shard_map/reduce_scatter | solution.py:280
  344.9 3.0 copy.573
  348.0 10.9 %all-to-all-start.2 = ((bf16[64,4,2048]{2,1,0:T(4,128)(2,1)}), bf16[64,4,2048]{2,1,0:T(4,128)(2,1)}, u32[]{:S(2)}, u32[]{:S(2)}) async-start(bf16[64,4,2048]{2,1,0:T(4,128)(2,1)} %copy.573), calls=%async_computation.3 | async-start | bytes 2097152 | tf_op jit(solution)/shard_map/all_to_all | solution.py:288
  359.4 27.5 %all-to-all-done.2 = bf16[64,4,2048]{2,1,0:T(4,128)(2,1)} async-done(((bf16[64,4,2048]{2,1,0:T(4,128)(2,1)}), bf16[64,4,2048]{2,1,0:T(4,128)(2,1)}, u32[]{:S(2)}, u32[]{:S(2)}) %all-to-all-start.2) | async-done | bytes 1048608 | tf_op jit(solution)/shard_map/all_to_all | solution.py:288
  387.0 1.3 reshape.915
  388.3 1.9 gather_fusion.1
  390.2 1.8 gather.15
  392.0 2.3 multiply_reduce_fusion.1
  (258 shorter events, 46.6 us)
Async XLA Ops:
  6.5 153.0 %copy-start = (bf16[256,2048]{1,0:T(8,128)(2,1)S(1)}, bf16[256,2048]{1,0:T(8,128)(2,1)}, u32[]{:S(2)}) copy-start(bf16[256,2048]{1,0:T(8,128)(2,1)} %param.28) | copy-start | bytes 3145732
  6.5 113.2 %copy-start.8 = (s32[256]{0:T(256)S(1)}, s32[256]{0:T(256)}, u32[]{:S(2)}) copy-start(s32[256]{0:T(256)} %param.27) | copy-start | bytes 3076
  6.5 112.5 %copy-start.5 = (f32[256,4]{0,1:T(4,128)S(1)}, f32[256,4]{0,1:T(4,128)}, u32[]{:S(2)}) copy-start(f32[256,4]{0,1:T(4,128)} %param.26) | copy-start | bytes 12292
  11.0 109.6 %copy-start.2 = (bf16[256,256]{1,0:T(8,128)(2,1)S(1)}, bf16[256,256]{1,0:T(8,128)(2,1)}, u32[]{:S(2)}) copy-start(bf16[256,256]{1,0:T(8,128)(2,1)} %param.22) | copy-start | bytes 393220
  16.7 110.1 %copy-start.4 = (bf16[256,128]{1,0:T(8,128)(2,1)S(1)}, bf16[256,128]{1,0:T(8,128)(2,1)}, u32[]{:S(2)}) copy-start(bf16[256,128]{1,0:T(8,128)(2,1)} %param.20) | copy-start | bytes 196612
  130.6 29.0 %copy-start.3 = (bf16[256,256]{1,0:T(8,128)(2,1)S(1)}, bf16[256,256]{1,0:T(8,128)(2,1)}, u32[]{:S(2)}) copy-start(bf16[256,256]{1,0:T(8,128)(2,1)} %param.23) | copy-start | bytes 393220
  158.8 6.4 %copy-start.9 = (s32[256,2]{0,1:T(2,128)S(1)}, s32[256,2]{0,1:T(2,128)}, u32[]{:S(2)}) copy-start(s32[256,2]{0,1:T(2,128)} %param.31) | copy-start | bytes 6148
  158.8 8.7 %copy-start.6 = (f32[2,2048]{1,0:T(2,128)S(1)}, f32[2,2048]{1,0:T(2,128)}, u32[]{:S(2)}) copy-start(f32[2,2048]{1,0:T(2,128)} %param.30) | copy-start | bytes 49156
  158.9 8.7 %copy-start.7 = (f32[2,2048]{1,0:T(2,128)S(1)}, f32[2,2048]{1,0:T(2,128)}, u32[]{:S(2)}) copy-start(f32[2,2048]{1,0:T(2,128)} %param.29) | copy-start | bytes 49156
  159.4 15.7 %copy-start.1 = (bf16[64,2048]{1,0:T(8,128)(2,1)S(1)}, bf16[64,2048]{1,0:T(8,128)(2,1)}, u32[]{:S(2)}) copy-start(bf16[64,2048]{1,0:T(8,128)(2,1)} %param.19) | copy-start | bytes 786436
  161.1 13.9 %all-to-all-start = ((bf16[4,64,2048]{2,1,0:T(8,128)(2,1)}), bf16[4,64,2048]{2,1,0:T(8,128)(2,1)S(1)}, u32[]{:S(2)}, u32[]{:S(2)}) async-start(bf16[4,64,2048]{2,1,0:T(8,128)(2,1)} %bitcast.115), calls=%async_computation | async-start | bytes 2097152 | tf_op jit(solution)/shard_map/all_to_all | solution.py:72
  165.3 106.5 %all-gather.8.cloned.1.call-start = ((), (), s32[]{:S(2)}) async-start(), calls=%async_computation.4 | async-start | bytes 5242880 | tf_op jit(solution)/shard_map/all_gather | solution.py:267
  225.9 119.0 %reduce-scatter.2.cloned.1.call-start = ((), (), s32[]{:S(2)}) async-start(), calls=%async_computation.5 | async-start | bytes 5242880 | tf_op jit(solution)/shard_map/reduce_scatter | solution.py:280
  271.7 4.6 %copy-start.11 = (bf16[1,2048,896]{2,1,0:T(8,128)(2,1)S(1)}, bf16[1,2048,896]{2,1,0:T(8,128)(2,1)}, u32[]{:S(2)}) copy-start(bf16[1,2048,896]{2,1,0:T(8,128)(2,1)} %param.34) | copy-start | bytes 11010052
  276.4 4.5 %copy-start.12 = (bf16[1,2048,896]{2,1,0:T(8,128)(2,1)S(1)}, bf16[1,2048,896]{2,1,0:T(8,128)(2,1)}, u32[]{:S(2)}) copy-start(bf16[1,2048,896]{2,1,0:T(8,128)(2,1)} %param.33) | copy-start | bytes 11010052
  280.9 4.8 %copy-start.13 = (bf16[1,896,2048]{2,1,0:T(8,128)(2,1)S(1)}, bf16[1,896,2048]{2,1,0:T(8,128)(2,1)}, u32[]{:S(2)}) copy-start(bf16[1,896,2048]{2,1,0:T(8,128)(2,1)} %param.35) | copy-start | bytes 11010052
  294.9 64.3 %copy-start.10 = (f32[256,2]{0,1:T(2,128)S(1)}, f32[256,2]{0,1:T(2,128)}, u32[]{:S(2)}) copy-start(f32[256,2]{0,1:T(2,128)} %param.32) | copy-start | bytes 6148
  348.0 39.0 %all-to-all-start.2 = ((bf16[64,4,2048]{2,1,0:T(4,128)(2,1)}), bf16[64,4,2048]{2,1,0:T(4,128)(2,1)}, u32[]{:S(2)}, u32[]{:S(2)}) async-start(bf16[64,4,2048]{2,1,0:T(4,128)(2,1)} %copy.573), calls=%async_computation.3 | async-start | bytes 2097152 | tf_op jit(solution)/shard_map/all_to_all | solution.py:288
Sparse Core Ops, SparseCore 0:
  226.0 45.6 all-gather.7
  295.0 49.8 reduce-scatter.1
where the time goes:
time: 404 us; the launch traced here: 402 us
  waiting for transfers between devices  131 us (32%)
  blocking collectives  81.1 us (20%)
  between operations  71.5 us (18%)
  local copies, waits for them, and re-layouts  53.7 us (13%)
  other arithmetic  29.1 us (7%)
  matrix products  18.4 us (5%)
  starting transfers between devices  15.1 us (4%)
    reduce_scatter x1, waiting for transfers between devices, on_device(): lax.psum_scatter(partial_value.reshape(sources, slot_count, model_width)....  50 us
    all_to_all x1, blocking collectives, on_device(): lax.all_to_all(outgoing, SP, split_axis=0, concat_axis=0, tiled=True)  46.3 us
    all_gather x1, waiting for transfers between devices, on_device(): lax.all_gather(lax.all_to_all(outgoing, SP, split_axis=0, concat_axis=0,...  45.8 us
    all_gather x3, blocking collectives, gathered_once(): both, at, found = (lax.all_gather(jnp.concatenate(lines), axis), 0, {})  34.8 us
    all_to_all x1, waiting for transfers between devices, on_device(): lax.all_to_all(summed.astype(jnp.bfloat16), SP, split_axis=0, concat_axis...  27.5 us
    all_to_all x1, starting transfers between devices, on_device(): lax.all_to_all(summed.astype(jnp.bfloat16), SP, split_axis=0, concat_axis...  10.9 us
    reduce_sum x4, other arithmetic, block_pass(): jnp.sum(query_block[:, None] * decay_pairs * key_blk[None, :], axis=-1)  10.3 us
  transfers between devices with their start and end apart: 4, of which 4 were waited for; matrix products, arithmetic and copies ran while one was open for 1% of the time, Pallas kernels for 0%

commit v1 on v0

v1 whole, which is shorter than its diff:
```python
import functools

import jax
import jax.numpy as jnp
from jax import lax
from jax.experimental import pallas as pl
from jax.experimental.pallas import tpu as pltpu
from jax.sharding import Mesh
from jax.sharding import PartitionSpec as P

SP = ("sp_0", "sp_1", "sp_2")
SP_TP = ("sp_0", "sp_1", "sp_2", "tp")
MESH = pl.DeviceIdType.MESH
F32 = jnp.float32
BF = jnp.bfloat16
LEVELS = (1, 2, 4, 8, 16, 32, 64, 128)

eps_rms = 1e-06
eps_layer = 1e-05
decay_norm = 16.0


def dot(a, b):
    return jnp.dot(a, b, preferred_element_type=F32)


def dot_nt(a, b):
    return lax.dot_general(a, b, (((1,), (1,)), ((), ())), preferred_element_type=F32)


def dot_tn(a, b):
    return lax.dot_general(a, b, (((0,), (0,)), ((), ())), preferred_element_type=F32)


def iota(shape, dim):
    return lax.broadcasted_iota(jnp.int32, shape, dim)


def three_parts(a):
    high = a.astype(BF)
    rest = a - high.astype(F32)
    mid = rest.astype(BF)
    low = (rest - mid.astype(F32)).astype(BF)
    return high, mid, low


def offsets(count):
    order = [0]
    for d in range(1, count // 2 + 1):
        order.append(d)
        if count - d != d:
            order.append(count - d)
    return order


def place(sizes):
    z, x, c, y = (lax.axis_index(a) for a in SP_TP)
    return z, x, c, y


def greet(partners):
    barrier = pltpu.get_barrier_semaphore()
    for partner in partners:
        pl.semaphore_signal(barrier, inc=1, device_id=partner, device_id_type=MESH)
    return barrier


def remote(src, dst, send_sem, recv_sem, device):
    copy = pltpu.make_async_remote_copy(
        src_ref=src,
        dst_ref=dst,
        send_sem=send_sem,
        recv_sem=recv_sem,
        device_id=device,
        device_id_type=MESH,
    )
    copy.start()
    return copy


def wait_bytes(ref, sem):
    pltpu.make_async_copy(ref, ref, sem).wait()


def level_reference(total, level):
    rows, width = total.shape
    if level >= 8:
        split = total.reshape(rows // (2 * level), 2 * level, width)
        return jnp.broadcast_to(split[:, level - 1 : level, :], split.shape).reshape(rows, width)
    split = total.reshape(rows // 8, 8, width)
    place_in = iota(split.shape, 1)
    row = split[:, level - 1 : level, :]
    for start in range(2 * level, 8, 2 * level):
        later = split[:, start + level - 1 : start + level, :]
        row = jnp.where(place_in >= start, later, row)
    return jnp.broadcast_to(row, split.shape).reshape(rows, width)


def message(state_t, decay_row, doc_row):
    high, mid, low = three_parts(decay_row)
    zeros = jnp.zeros((12, decay_row.shape[1]), F32)
    tail = jnp.concatenate(
        [high.astype(F32), mid.astype(F32), low.astype(F32), doc_row, zeros], axis=0
    )
    return jnp.concatenate([state_t.astype(BF), tail.astype(BF)], axis=0)


def opened(buffer, k, width):
    block = buffer[k].astype(F32)
    state = block[:width]
    decay = block[width : width + 1] + block[width + 1 : width + 2] + block[width + 2 : width + 3]
    return state, decay, block[width + 3 : width + 4]


def attention_kernel(
    sizes,
    q_ref,
    k_ref,
    v_ref,
    g_ref,
    dgi_ref,
    off_ref,
    spk_ref,
    doc_ref,
    wo_ref,
    res_ref,
    gain_ref,
    shift_ref,
    out_ref,
    msg1,
    buf1,
    msg2,
    buf2,
    ql,
    kl,
    vh_ref,
    oacc,
    pb,
    far,
    near,
    summed,
    send1,
    recv1,
    send2,
    recv2,
    send3,
    recv3,
):
    zs, xs, cs, ys = sizes
    z, x, c, y = place(sizes)
    group = xs * cs
    me = x * cs + c
    peers = [
        (z, lax.rem(x + dx, xs), lax.rem(c + dc, cs), y)
        for dx in range(xs)
        for dc in range(cs)
        if dx or dc
    ]
    columns = [(lax.rem(z + dz, zs), x, c, y) for dz in offsets(zs)[1:]]
    plus = (z, x, c, lax.rem(y + 1, ys))
    minus = (z, x, c, lax.rem(y + ys - 1, ys))
    barrier = greet(peers + columns + [plus, minus])

    length, hk = q_ref.shape
    hv = v_ref.shape[1]
    heads = spk_ref.shape[1]
    dk = hk // heads
    dv = hv // heads
    lane_head = iota((1, hk), 1) // dk
    vlane_head = iota((1, hv), 1) // dv

    pre = dgi_ref[...].astype(F32) + off_ref[...]
    rate = -(jnp.maximum(-pre, 0.0) + jnp.log1p(jnp.exp(-jnp.abs(pre)))) / decay_norm
    spikes = spk_ref[...]
    for h in range(heads):
        rate = rate + jnp.where(lane_head == h, spikes[:, h : h + 1], 0.0)
    row_i = iota((length, length), 0)
    col_i = iota((length, length), 1)
    tri = (row_i >= col_i).astype(BF)
    high, mid, low = three_parts(rate)
    total = dot(tri, high) + dot(tri, mid) + dot(tri, low)
    last_total = total[length - 1 : length]

    doc_row = doc_ref[...].astype(F32)
    doc_col = jnp.sum(jnp.where(row_i == col_i, doc_row, 0.0), axis=1, keepdims=True)
    last_doc = doc_col[length - 1 : length]
    last_row = jnp.broadcast_to(last_doc, (1, hk))

    keys = k_ref[...].astype(F32)
    query = q_ref[...].astype(F32) * dk ** (-0.5)
    ends = keys * jnp.exp(jnp.minimum(last_total - total, 0.0))
    ends = jnp.where(doc_col == last_doc, ends, 0.0).astype(BF)
    cross = dot_tn(v_ref[...], ends)
    state_t = jnp.zeros((dv, hk), F32)
    for h in range(heads):
        state_t = state_t + jnp.where(lane_head == h, cross[h * dv : (h + 1) * dv], 0.0)
    first = message(state_t, last_total, last_row)
    msg1[...] = first
    buf1[me] = first
    pl.semaphore_wait(barrier, len(peers) + len(columns) + 2)
    for peer in peers:
        remote(msg1, buf1.at[me], send1, recv1, peer)

    ql[0] = query.astype(BF)
    kl[0] = keys.astype(BF)
    for n, level in enumerate(LEVELS):
        mark = level_reference(total, level)
        ql[n + 1] = (query * jnp.exp(jnp.minimum(total - mark, 0.0))).astype(BF)
        kl[n + 1] = (keys * jnp.exp(jnp.minimum(mark - total, 0.0))).astype(BF)
    entering = (query * jnp.exp(jnp.minimum(total, 0.0))).astype(BF)
    vh_ref[...] = v_ref[...]
    oacc[...] = jnp.zeros_like(oacc)
    visible = (row_i >= col_i) & (doc_col == doc_row)
    differ = row_i ^ col_i

    def head_work(h, carry):
        keep = lane_head == h
        scores = dot_nt(ql[0], jnp.where(keep, kl[0], jnp.zeros((), BF)))
        for n, level in enumerate(LEVELS):
            at_level = dot_nt(ql[n + 1], jnp.where(keep, kl[n + 1], jnp.zeros((), BF)))
            scores = jnp.where(differ >= level, at_level, scores)
        scores = jnp.where(visible, scores, 0.0).astype(BF)
        oacc[...] += dot(scores, jnp.where(vlane_head == h, v_ref[...], jnp.zeros((), BF)))
        return carry

    lax.fori_loop(0, heads // 2, head_work, 0)

    if group > 1:
        wait_bytes(buf1.at[pl.ds(0, group - 1)], recv1)
    last_of_group = None
    parts = [opened(buf1, j, dv) for j in range(group)]
    group_doc = parts[group - 1][2]
    mine_doc = jnp.full((1, hk), -1.0, F32)
    for j in range(group - 1):
        mine_doc = jnp.where(me == j + 1, parts[j][2], mine_doc)
    group_state = jnp.zeros((dv, hk), F32)
    within = jnp.zeros((dv, hk), F32)
    group_decay = jnp.zeros((1, hk), F32)
    own_decay = jnp.zeros((1, hk), F32)
    for j in range(group - 1, -1, -1):
        state_j, decay_j, doc_j = parts[j]
        share = jnp.where(doc_j == group_doc, jnp.exp(jnp.minimum(group_decay, 0.0)), 0.0)
        group_state = group_state + share * state_j
        group_decay = group_decay + decay_j
        earlier = j < me
        share = jnp.where(doc_j == mine_doc, jnp.exp(jnp.minimum(own_decay, 0.0)), 0.0)
        within = within + jnp.where(earlier, share, 0.0) * state_j
        own_decay = own_decay + jnp.where(earlier, decay_j, 0.0)
    second = message(group_state, group_decay, group_doc)
    msg2[...] = second
    buf2[z] = second
    for peer in columns:
        remote(msg2, buf2.at[z], send2, recv2, peer)

    lax.fori_loop(heads // 2, heads, head_work, 0)

    gate = g_ref[...].astype(F32)
    gate = gate / (1.0 + jnp.exp(-gate))

    if zs > 1:
        wait_bytes(buf2.at[pl.ds(0, zs - 1)], recv2)
    parts = [opened(buf2, k, dv) for k in range(zs)]
    for k in range(zs - 1):
        mine_doc = jnp.where((me == 0) & (z == k + 1), parts[k][2], mine_doc)
    for k in range(zs - 1, -1, -1):
        state_k, decay_k, doc_k = parts[k]
        earlier = k < z
        share = jnp.where(doc_k == mine_doc, jnp.exp(jnp.minimum(own_decay, 0.0)), 0.0)
        within = within + jnp.where(earlier, share, 0.0) * state_k
        own_decay = own_decay + jnp.where(earlier, decay_k, 0.0)
    arriving = jnp.concatenate(
        [jnp.where(lane_head == h, within, 0.0).astype(BF) for h in range(heads)], axis=0
    )
    carried = dot_nt(entering, arriving)
    carried = jnp.where(doc_col == mine_doc[:, 0:1], carried, 0.0)
    recurrent = oacc[...] + carried
    same = (iota((hv, hv), 0) // dv == iota((hv, hv), 1) // dv).astype(BF)
    square = recurrent * recurrent
    square_high = square.astype(BF)
    square_low = (square - square_high.astype(F32)).astype(BF)
    mean = (dot(square_high, same) + dot(square_low, same)) / dv
    mixed = (recurrent * lax.rsqrt(mean + eps_rms) * gate).astype(BF)

    width = wo_ref.shape[1]
    tile = width // 4
    for n in range(4):
        pb[:, n * tile : (n + 1) * tile] = dot(
            mixed, wo_ref[:, n * tile : (n + 1) * tile]
        ).astype(BF)

    rows = length // ys
    half = rows // 2

    def mine(offset, start):
        base = lax.rem(y + offset, ys) * rows + start
        return pb.at[pl.ds(pl.multiple_of(base, half), half)]

    remote(mine(2, 0), far.at[0], send3.at[0], recv3.at[0], minus)
    remote(mine(2, half), far.at[1], send3.at[1], recv3.at[1], plus)
    remote(mine(ys - 1, half), near.at[0, 1], send3.at[2], recv3.at[2], minus)
    remote(mine(1, 0), near.at[1, 0], send3.at[3], recv3.at[3], plus)
    wait_bytes(far.at[0], recv3.at[0])
    summed[0] = (mine(ys - 1, 0)[...].astype(F32) + far[0].astype(F32)).astype(BF)
    remote(summed.at[0], near.at[0, 0], send3.at[4], recv3.at[4], minus)
    wait_bytes(far.at[1], recv3.at[1])
    summed[1] = (mine(1, half)[...].astype(F32) + far[1].astype(F32)).astype(BF)
    remote(summed.at[1], near.at[1, 1], send3.at[5], recv3.at[5], plus)
    gain = gain_ref[0:1, :]
    shift = shift_ref[0:1, :]
    wait_bytes(near.at[0, 1], recv3.at[2])
    wait_bytes(near.at[1, 0], recv3.at[3])
    wait_bytes(near.at[0, 0], recv3.at[4])
    wait_bytes(near.at[1, 1], recv3.at[5])
    for s in range(2):
        stream = res_ref[s * half : (s + 1) * half].astype(F32)
        stream = stream + mine(0, s * half)[...].astype(F32)
        stream = stream + near[0, s].astype(F32) + near[1, s].astype(F32)
        center = jnp.mean(stream, axis=-1, keepdims=True)
        moved = stream - center
        spread = jnp.mean(moved * moved, axis=-1, keepdims=True)
        out_ref[s * half : (s + 1) * half] = (
            moved * lax.rsqrt(spread + eps_layer) * gain + shift
        ).astype(BF)
    if group > 1:
        wait_bytes(buf1.at[pl.ds(0, group - 1)], send1)
    if zs > 1:
        wait_bytes(buf2.at[pl.ds(0, zs - 1)], send2)
    for n in range(6):
        wait_bytes(far.at[0], send3.at[n])


def attention(sizes, *args):
    q, v, residual, heads = args[0], args[2], args[9], args[6].shape[1]
    zs, xs, cs, ys = sizes
    length, hk = q.shape
    hv = v.shape[1]
    dv = hv // heads
    rows, width = residual.shape
    group = xs * cs
    dma = pltpu.SemaphoreType.DMA
    return pl.pallas_call(
        functools.partial(attention_kernel, sizes),
        out_shape=jax.ShapeDtypeStruct((rows, width), BF),
        in_specs=[pl.BlockSpec(memory_space=pltpu.VMEM)] * len(args),
        out_specs=pl.BlockSpec(memory_space=pltpu.VMEM),
        scratch_shapes=[
            pltpu.VMEM((dv + 16, hk), BF),
            pltpu.VMEM((group, dv + 16, hk), BF),
            pltpu.VMEM((dv + 16, hk), BF),
            pltpu.VMEM((zs, dv + 16, hk), BF),
            pltpu.VMEM((len(LEVELS) + 1, length, hk), BF),
            pltpu.VMEM((len(LEVELS) + 1, length, hk), BF),
            pltpu.VMEM((length, hv), BF),
            pltpu.VMEM((length, hv), F32),
            pltpu.VMEM((length, width), BF),
            pltpu.VMEM((2, rows // 2, width), BF),
            pltpu.VMEM((2, 2, rows // 2, width), BF),
            pltpu.VMEM((2, rows // 2, width), BF),
            dma,
            dma,
            dma,
            dma,
            dma((6,)),
            dma((6,)),
        ],
        compiler_params=pltpu.CompilerParams(
            collective_id=0, has_side_effects=True, vmem_limit_bytes=40 * 1024 * 1024
        ),
        name="attention",
    )(*args)


def experts_kernel(
    sizes,
    normed_ref,
    routes_ref,
    weights_ref,
    gain_ref,
    shift_ref,
    wg_hbm,
    wu_hbm,
    wd_hbm,
    out_ref,
    wg,
    wu,
    wd,
    stack,
    outb,
    inb,
    xg,
    hid,
    yb,
    ra,
    rs,
    rb,
    backb,
    retb,
    wsem,
    dsend,
    drecv,
    gsend,
    grecv,
    fsend,
    frecv,
    asend,
    arecv,
    nsend,
    nrecv,
    ssend,
    srecv,
    bsend,
    brecv,
):
    zs, xs, cs, ys = sizes
    z, x, c, y = place(sizes)
    group = xs * cs
    me = x * cs + c
    steps = offsets(zs)
    around = [(dx, dc) for dx in range(xs) for dc in range(cs)]
    plus = (z, x, c, lax.rem(y + 1, ys))
    minus = (z, x, c, lax.rem(y + ys - 1, ys))

    def peer(dz, dx, dc):
        return (lax.rem(z + dz, zs), lax.rem(x + dx, xs), lax.rem(c + dc, cs), y)

    partners = [
        peer(dz, dx, dc) for dz in range(zs) for dx, dc in around if dz or dx or dc
    ]
    barrier = greet(partners + [plus, minus])
    loads = [
        pltpu.make_async_copy(src.at[0], dst, wsem.at[n])
        for n, (src, dst) in enumerate(((wg_hbm, wg), (wu_hbm, wu), (wd_hbm, wd)))
    ]
    for load in loads:
        load.start()

    rows, model = normed_ref.shape
    cols = model // 4
    spots = group * 16
    keep = group * 4

    start = pl.multiple_of(y * rows, rows)
    own_routes = routes_ref[pl.ds(start, rows), :]
    own_weights = weights_ref[pl.ds(start, rows), :]
    experts = zs * group
    marks = [
        (own_routes[:, j : j + 1] == iota((rows, experts), 1)).astype(F32) for j in range(2)
    ]
    below = (iota((rows, rows), 0) > iota((rows, rows), 1)).astype(BF)
    before = dot(below, marks[0].astype(BF))
    pos0 = jnp.sum(before * marks[0], axis=1, keepdims=True)
    before = dot(below, marks[1].astype(BF)) + jnp.sum(marks[0], axis=0, keepdims=True)
    pos1 = jnp.sum(before * marks[1], axis=1, keepdims=True)
    quarter = iota((4 * rows, 1), 0) // rows * 4
    slot_cols = []
    slot_rows = []
    square = iota((4 * rows, 4 * rows), 0) == iota((4 * rows, 4 * rows), 1)
    for j, pos in ((0, pos0), (1, pos1)):
        one = own_routes[:, j : j + 1] * 16 + pos.astype(jnp.int32)
        one = jnp.concatenate([one] * 4, axis=0) + quarter
        slot_cols.append(one)
        as_row = jnp.sum(jnp.where(square, one.astype(F32), 0.0), axis=0, keepdims=True)
        slot_rows.append(as_row.astype(jnp.int32))
    weight_cols = [
        jnp.concatenate([own_weights[:, j : j + 1]] * 4, axis=0) for j in range(2)
    ]

    for n in range(4):
        stack[n * rows : (n + 1) * rows] = normed_ref[:, n * cols : (n + 1) * cols]

    def spot_ids(shape, dim, dz):
        return iota(shape, dim) + lax.rem(z + dz, zs) * spots

    to_rows = iota((spots, spots), 0)
    from_rows = iota((spots, spots), 1)
    arranged = (to_rows % keep // 4) * 16 + (to_rows // keep) * 4 + to_rows % 4
    arrange = (from_rows == arranged).astype(BF)
    arranged = (from_rows % keep // 4) * 16 + (from_rows // keep) * 4 + from_rows % 4
    restore = (to_rows == arranged).astype(BF)

    for k, dz in enumerate(steps):
        ids = spot_ids((spots, 4 * rows), 0, dz)
        pick = ((ids == slot_rows[0]) | (ids == slot_rows[1])).astype(BF)
        outb[k] = dot(pick, stack[...]).astype(BF)
        if k == 0:
            pl.semaphore_wait(barrier, len(partners) + 2)
        for dx, dc in around:
            to = peer(dz, dx, dc)
            target = to[1] * cs + to[2]
            source = outb.at[k, pl.ds(pl.multiple_of(target * 16, 16), 16)]
            landing = inb.at[k, pl.ds(pl.multiple_of(me * 16, 16), 16)]
            if dz or dx or dc:
                remote(source, landing, dsend.at[k], drecv.at[k], to)
            else:
                landing[...] = source[...]

    def sized(buffer, k, dz):
        count = spots if dz else spots - 16
        return buffer.at[k, pl.ds(0, count)]

    halves = keep // 2

    def forward(k):
        wait_bytes(xg.at[k, 1], grecv.at[k, 0])
        remote(
            xg.at[k, 1, pl.ds(0, halves)],
            xg.at[k, 2, pl.ds(0, halves)],
            fsend.at[k, 0],
            frecv.at[k, 0],
            plus,
        )
        wait_bytes(xg.at[k, 3], grecv.at[k, 1])
        remote(
            xg.at[k, 3, pl.ds(halves, halves)],
            xg.at[k, 2, pl.ds(halves, halves)],
            fsend.at[k, 1],
            frecv.at[k, 1],
            minus,
        )

    for k, dz in enumerate(steps):
        if (spots if dz else spots - 16) > 0:
            wait_bytes(sized(inb, k, dz), drecv.at[k])
        tidy = dot(arrange, inb[k]).astype(BF)
        for n in range(4):
            xg[k, 0, :, n * cols : (n + 1) * cols] = tidy[n * keep : (n + 1) * keep]
        remote(xg.at[k, 0], xg.at[k, 1], gsend.at[k, 0], grecv.at[k, 0], plus)
        remote(xg.at[k, 0], xg.at[k, 3], gsend.at[k, 1], grecv.at[k, 1], minus)
        if k:
            forward(k - 1)
    forward(zs - 1)

    units = wg.shape[1]
    tiles = [(n, min(256, units - n)) for n in range(0, units, 256)]
    bundle = 2 if zs == 2 else zs // 2

    def back(k, dz):
        wait_bytes(ra.at[k, 0], arecv.at[k, 0])
        rs[k, 0] = (yb[k, 1, 0:halves].astype(F32) + ra[k, 0].astype(F32)).astype(BF)
        remote(rs.at[k, 0], rb.at[k, 0, pl.ds(0, halves)], ssend.at[k, 0], srecv.at[k, 0], minus)
        wait_bytes(ra.at[k, 1], arecv.at[k, 1])
        rs[k, 1] = (yb[k, 3, halves:keep].astype(F32) + ra[k, 1].astype(F32)).astype(BF)
        remote(
            rs.at[k, 1], rb.at[k, 1, pl.ds(halves, halves)], ssend.at[k, 1], srecv.at[k, 1], plus
        )

    def finish(k, dz):
        wait_bytes(rb.at[k, 0, pl.ds(halves, halves)], nrecv.at[k, 0])
        wait_bytes(rb.at[k, 1, pl.ds(0, halves)], nrecv.at[k, 1])
        wait_bytes(rb.at[k, 0, pl.ds(0, halves)], srecv.at[k, 0])
        wait_bytes(rb.at[k, 1, pl.ds(halves, halves)], srecv.at[k, 1])
        whole = yb[k, 0].astype(F32) + rb[k, 0].astype(F32) + rb[k, 1].astype(F32)
        whole = whole.astype(BF)
        laid = jnp.concatenate(
            [whole[:, n * cols : (n + 1) * cols] for n in range(4)], axis=0
        )
        backb[k] = dot(restore, laid).astype(BF)
        for dx, dc in around:
            to = peer((zs - dz) % zs, dx, dc)
            target = to[1] * cs + to[2]
            source = backb.at[k, pl.ds(pl.multiple_of(target * 16, 16), 16)]
            landing = retb.at[k, pl.ds(pl.multiple_of(me * 16, 16), 16)]
            if dz or dx or dc:
                remote(source, landing, bsend.at[k], brecv.at[k], to)
            else:
                landing[...] = source[...]

    for first in range(0, zs, bundle):
        chunk = range(first, first + bundle)
        for k in chunk:
            wait_bytes(xg.at[k, 2, pl.ds(0, halves)], frecv.at[k, 0])
            wait_bytes(xg.at[k, 2, pl.ds(halves, halves)], frecv.at[k, 1])
        if first == 0:
            loads[0].wait()
            loads[1].wait()
        big = bundle * ys * keep

        def gate_up(at, size):
            block = xg[first : first + bundle].reshape(big, model)
            gate = dot(block, wg[:, pl.ds(at, size)])
            up = dot(block, wu[:, pl.ds(at, size)])
            hid[:, pl.ds(at, size)] = (gate / (1.0 + jnp.exp(-gate)) * up).astype(BF)

        for at, size in tiles:
            gate_up(at, size)
        if first == 0:
            loads[2].wait()
        for at in range(0, model, 256):
            part = dot(hid[...], wd[:, at : at + 256]).astype(BF)
            yb[first : first + bundle, :, :, at : at + 256] = part.reshape(bundle, ys, keep, 256)
        for k in chunk:
            remote(yb.at[k, 2, pl.ds(0, halves)], ra.at[k, 0], asend.at[k, 0], arecv.at[k, 0], minus)
            remote(
                yb.at[k, 2, pl.ds(halves, halves)], ra.at[k, 1], asend.at[k, 1], arecv.at[k, 1], plus
            )
            remote(
                yb.at[k, 1, pl.ds(halves, halves)],
                rb.at[k, 0, pl.ds(halves, halves)],
                nsend.at[k, 0],
                nrecv.at[k, 0],
                minus,
            )
            remote(
                yb.at[k, 3, pl.ds(0, halves)],
                rb.at[k, 1, pl.ds(0, halves)],
                nsend.at[k, 1],
                nrecv.at[k, 1],
                plus,
            )
    for k, dz in enumerate(steps):
        back(k, dz)
        if k:
            finish(k - 1, steps[k - 1])
    finish(zs - 1, steps[-1])

    mix = jnp.zeros((4 * rows, cols), F32)
    for k, dz in enumerate(steps):
        if (spots if dz else spots - 16) > 0:
            wait_bytes(sized(retb, k, dz), brecv.at[k])
        ids = spot_ids((4 * rows, spots), 1, dz)
        share = jnp.where(ids == slot_cols[0], weight_cols[0], 0.0)
        share = share + jnp.where(ids == slot_cols[1], weight_cols[1], 0.0)
        high = share.astype(BF)
        low = (share - high.astype(F32)).astype(BF)
        mix = mix + dot(high, retb[k]) + dot(low, retb[k])
    mix = mix + stack[...].astype(F32)
    pieces = [mix[n * rows : (n + 1) * rows] for n in range(4)]
    center = sum(jnp.sum(piece, axis=1, keepdims=True) for piece in pieces) / model
    pieces = [piece - center for piece in pieces]
    spread = sum(jnp.sum(piece * piece, axis=1, keepdims=True) for piece in pieces) / model
    scale = lax.rsqrt(spread + eps_layer)
    for n in range(4):
        lanes = slice(n * cols, (n + 1) * cols)
        out_ref[:, lanes] = (
            pieces[n] * scale * gain_ref[1:2, lanes] + shift_ref[1:2, lanes]
        ).astype(BF)

    for k, dz in enumerate(steps):
        if (spots if dz else spots - 16) > 0:
            wait_bytes(sized(outb, k, dz), dsend.at[k])
            wait_bytes(sized(backb, k, dz), bsend.at[k])
        for n in range(2):
            wait_bytes(xg.at[k, 0], gsend.at[k, n])
            half = xg.at[k, 0, pl.ds(0, halves)]
            for sem in (fsend, asend, nsend, ssend):
                wait_bytes(half, sem.at[k, n])


def routed(sizes, *args):
    normed, wg = args[0], args[5]
    zs, xs, cs, ys = sizes
    rows, model = normed.shape
    units = wg.shape[2]
    group = xs * cs
    spots, keep, cols = group * 16, group * 4, model // 4
    bundle = 2 if zs == 2 else zs // 2
    dma = pltpu.SemaphoreType.DMA
    vmem = pl.BlockSpec(memory_space=pltpu.VMEM)
    hbm = pl.BlockSpec(memory_space=pl.ANY)
    return pl.pallas_call(
        functools.partial(experts_kernel, sizes),
        out_shape=jax.ShapeDtypeStruct((rows, model), BF),
        in_specs=[vmem] * 5 + [hbm] * 3,
        out_specs=vmem,
        scratch_shapes=[
            pltpu.VMEM((model, units), BF),
            pltpu.VMEM((model, units), BF),
            pltpu.VMEM((units, model), BF),
            pltpu.VMEM((4 * rows, cols), BF),
            pltpu.VMEM((zs, spots, cols), BF),
            pltpu.VMEM((zs, spots, cols), BF),
            pltpu.VMEM((zs, ys, keep, model), BF),
            pltpu.VMEM((bundle * ys * keep, units), BF),
            pltpu.VMEM((zs, ys, keep, model), BF),
            pltpu.VMEM((zs, 2, keep // 2, model), BF),
            pltpu.VMEM((zs, 2, keep // 2, model), BF),
            pltpu.VMEM((zs, 2, keep, model), BF),
            pltpu.VMEM((zs, spots, cols), BF),
            pltpu.VMEM((zs, spots, cols), BF),
            dma((3,)),
            dma((zs,)),
            dma((zs,)),
        ]
        + [dma((zs, 2))] * 10
        + [dma((zs,)), dma((zs,))],
        compiler_params=pltpu.CompilerParams(
            collective_id=1, has_side_effects=True, vmem_limit_bytes=60 * 1024 * 1024
        ),
        name="experts",
    )(*args)


def on_device(
    sizes,
    residual,
    queries,
    projected_keys,
    values,
    projected_output_gate,
    decay_gate_input,
    decay_gate_offset,
    decay_spikes,
    documents,
    attention_output_weight,
    layer_norm_gains,
    layer_norm_shifts,
    routes,
    chosen_expert_weights,
    expert_gate_weight,
    expert_up_weight,
    expert_down_weight,
):
    normed = attention(
        sizes,
        queries,
        projected_keys,
        values,
        projected_output_gate,
        decay_gate_input,
        decay_gate_offset.reshape(1, -1),
        decay_spikes,
        documents.reshape(1, -1),
        attention_output_weight,
        residual,
        layer_norm_gains,
        layer_norm_shifts,
    )
    return routed(
        sizes,
        normed,
        routes,
        chosen_expert_weights,
        layer_norm_gains,
        layer_norm_shifts,
        expert_gate_weight,
        expert_up_weight,
        expert_down_weight,
    )


def build(torus):
    sizes = tuple(torus.shape[a] for a in SP_TP)
    return jax.shard_map(
        functools.partial(on_device, sizes),
        mesh=torus,
        in_specs=(
            P(SP_TP, None),
            P(SP, "tp"),
            P(SP, "tp"),
            P(SP, "tp"),
            P(SP, "tp"),
            P(SP, "tp"),
            P("tp"),
            P(SP, "tp"),
            P(SP),
            P("tp", None),
            P(),
            P(),
            P(SP, None),
            P(SP, None),
            P(SP, None, "tp"),
            P(SP, None, "tp"),
            P(SP, "tp", None),
        ),
        out_specs=P(SP_TP, None),
        check_vma=False,
    )


def solution(mesh):
    return build(Mesh(mesh.devices.reshape(8, 4, 2, mesh.shape["tp"]), SP_TP))
```

time: 404 us -> 163 us (0.40)
  Pallas kernels: 0 us -> 147 us
  waiting for transfers between devices: 131 us -> 0 us
  blocking collectives: 81.1 us -> 0 us
  between operations: 71.5 us -> 0.05 us
  local copies, waits for them, and re-layouts: 53.7 us -> 15.4 us
  other arithmetic: 29.1 us -> 0 us
  matrix products: 18.4 us -> 0 us
  starting transfers between devices: 15.1 us -> 0 us
    pallas_call x0 -> x2, Pallas kernels: none -> 147 us  [the longest x1 117 us: routed(): pl.pallas_call(functools.partial(experts_kernel, sizes), out_shape=jax.Sh...]
    reduce_scatter x1 -> x0, waiting for transfers between devices: 50 us -> none  [on_device(): lax.psum_scatter(partial_value.reshape(sources, slot_count, model_width)....]
    all_to_all x1 -> x0, blocking collectives: 46.3 us -> none  [on_device(): lax.all_to_all(outgoing, SP, split_axis=0, concat_axis=0, tiled=True)]
    all_gather x1 -> x0, waiting for transfers between devices: 45.8 us -> none  [on_device(): lax.all_gather(lax.all_to_all(outgoing, SP, split_axis=0, concat_axis=0,...]
    all_to_all x2 -> x0, waiting for transfers between devices: 34.9 us -> none  [the longest x1 27.5 us: on_device(): lax.all_to_all(summed.astype(jnp.bfloat16), SP, split_axis=0, concat_axis...]
    all_gather x3 -> x0, blocking collectives: 34.8 us -> none  [gathered_once(): both, at, found = (lax.all_gather(jnp.concatenate(lines), axis), 0, {})]
    dot_general x17 -> x0, matrix products: 18.4 us -> none  [the longest x1 4.95 us: expert_quarter(): jnp.dot(hidden, down_part, preferred_element_type=jnp.float32)]
    all_to_all x2 -> x0, starting transfers between devices: 15.1 us -> none  [the longest x1 10.9 us: on_device(): lax.all_to_all(summed.astype(jnp.bfloat16), SP, split_axis=0, concat_axis...]
  transfers between devices with their start and end apart: 4 -> 0, of which waited for: 4 -> 0; matrix products, arithmetic and copies ran while one was open for 1% -> 0% of each run, Pallas kernels for 0% -> 0%
where the time goes in v1:
time: 163 us; the launch traced here: 162 us
  Pallas kernels  147 us (90%)
  local copies, waits for them, and re-layouts  15.4 us (9%)
    pallas_call x1, Pallas kernels, routed(): pl.pallas_call(functools.partial(experts_kernel, sizes), out_shape=jax.Sh...  117 us
    pallas_call x1, Pallas kernels, attention(): pl.pallas_call(functools.partial(attention_kernel, sizes), out_shape=jax....  29.9 us
    unnamed x28, local copies, waits for them, and re-layouts  15.4 us

profile of v1, /device:TPU:1, one launch (start us, length us, event | category | flops | bytes accessed | tf_op | source)
XLA Modules:
  0.0 162.0 jit_solution(16650889106971775408)
XLA Ops:
  0.0 0.8 copy.18.spk_ref
  0.8 0.0 copy-start.1
  0.8 1.2 copy-done.1
  2.1 0.0 copy-start.2
  2.1 0.9 copy-done.2
  3.0 0.0 copy-start.3
  3.0 0.9 copy-done.3
  3.9 0.0 copy-start.4
  3.9 0.9 copy-done.4
  4.8 0.0 copy-start.5
  4.8 0.7 copy-done.5
  5.5 0.0 copy-start.6
  5.5 0.7 copy-done.6
  6.2 0.0 copy-start.7
  6.2 0.8 copy-done.7
  7.1 0.0 copy-start.8
  7.1 0.8 copy-done.8
  7.9 0.0 copy-start.9
  7.9 0.8 copy-done.9
  8.8 0.0 copy-start.10
  8.8 0.7 copy-done.10
  9.4 0.0 copy-start.11
  9.4 0.7 copy-done.11
  10.1 29.9 %attention.1.normed_ref = bf16[64,2048]{1,0:T(8,128)(2,1)S(1)} custom-call(bf16[256,128]{1,0:T(8,128)(2,1)S(1)} %copy-done.7, bf16[256,128]{1,0:T(8,128)(2,1)S(1)} %copy-done.8, bf16[256,256]{1,0:T(8,128)(2,1)S(1)} %copy-done.3, bf16[256,256]{1,0:T(8,128)(2,1)S(1)} %copy-done.4, bf16[256,128]{1,0:T(8,128)(2,1)S(1)} %copy-done.9, f32[1,128]{1,0:T(1,128)S(1)} %bitcast.3, ...), custom_call_target="tpu_custom_call" | custom-call | tf_op jit(solution)/shard_map/attention/pallas_call | solution.py:341
  40.0 0.0 copy-start
  40.0 0.7 copy-done
  40.7 1.5 copy.19.routes_ref
  42.2 1.5 copy.20.weights_ref
  43.6 116.7 %experts.1 = bf16[64,2048]{1,0:T(8,128)(2,1)} custom-call(bf16[64,2048]{1,0:T(8,128)(2,1)} %copy-done, s32[256,2]{1,0:T(8,128)} %copy.19.routes_ref, f32[256,2]{1,0:T(8,128)} %copy.20.weights_ref, f32[2,2048]{1,0:T(2,128)} %gain_ref.3, f32[2,2048]{1,0:T(2,128)} %shift_ref.3, bf16[1,2048,896]{2,1,0:T(8,128)(2,1)} %wg_hbm.1, bf16[1,2048,896]{2,1,0:T(8,128)(2,1)} %wu_hbm.1, ...), custom_call_target="tpu_custom_call" | custom-call | tf_op jit(solution)/shard_map/experts/pallas_call | solution.py:660
  160.3 1.7 %copy.22 = bf16[64,2048]{1,0:T(8,128)(2,1)} copy(bf16[64,2048]{1,0:T(8,128)(2,1)} %experts.1) | data formatting | bytes 524288
Async XLA Ops:
  0.8 1.2 copy-start.1
  2.1 0.9 copy-start.2
  3.0 0.9 copy-start.3
  3.9 0.9 copy-start.4
  4.8 0.7 copy-start.5
  5.5 0.7 copy-start.6
  6.2 0.8 copy-start.7
  7.1 0.8 copy-start.8
  7.9 0.8 copy-start.9
  8.8 0.7 copy-start.10
  9.4 0.7 copy-start.11
  40.0 0.7 copy-start

commit v2 on v1

v2 whole, which is shorter than its diff:
```python
import functools

import jax
import jax.numpy as jnp
from jax import lax
from jax.experimental import pallas as pl
from jax.experimental.pallas import tpu as pltpu
from jax.sharding import Mesh
from jax.sharding import PartitionSpec as P

SP = ("sp_0", "sp_1", "sp_2")
SP_TP = ("sp_0", "sp_1", "sp_2", "tp")
MESH = pl.DeviceIdType.MESH
F32 = jnp.float32
BF = jnp.bfloat16
LAGS = (2, 3, 4, 6)
LEVELS = (1, 2, 4, 8, 16, 32, 64, 128)

eps_rms = 1e-06
eps_layer = 1e-05
decay_norm = 16.0


def dot(a, b):
    return jnp.dot(a, b, preferred_element_type=F32)


def dot_nt(a, b):
    return lax.dot_general(a, b, (((1,), (1,)), ((), ())), preferred_element_type=F32)


def dot_tn(a, b):
    return lax.dot_general(a, b, (((0,), (0,)), ((), ())), preferred_element_type=F32)


def iota(shape, dim):
    return lax.broadcasted_iota(jnp.int32, shape, dim)


def three_parts(a):
    high = a.astype(BF)
    rest = a - high.astype(F32)
    mid = rest.astype(BF)
    low = (rest - mid.astype(F32)).astype(BF)
    return high, mid, low


def offsets(count):
    order = [0]
    for d in range(1, count // 2 + 1):
        order.append(d)
        if count - d != d:
            order.append(count - d)
    return order


def plan(zs):
    direct = (0, 1, zs - 1) if zs >= 4 else (0,)
    steps = [2, 6, 3, 1, 5, 7, 4, 0] if zs == 8 else offsets(zs)[::-1]
    first = [k for k, dz in enumerate(steps) if dz not in direct]
    late = [k for k, dz in enumerate(steps) if dz in direct]
    return steps, first, late


def place(sizes):
    z, x, c, y = (lax.axis_index(a) for a in SP_TP)
    return z, x, c, y


def greet(partners):
    barrier = pltpu.get_barrier_semaphore()
    for partner in partners:
        pl.semaphore_signal(barrier, inc=1, device_id=partner, device_id_type=MESH)
    return barrier


def remote(src, dst, send_sem, recv_sem, device):
    copy = pltpu.make_async_remote_copy(
        src_ref=src,
        dst_ref=dst,
        send_sem=send_sem,
        recv_sem=recv_sem,
        device_id=device,
        device_id_type=MESH,
    )
    copy.start()
    return copy


def wait_bytes(ref, sem):
    pltpu.make_async_copy(ref, ref, sem).wait()


def level_reference(total, level):
    rows, width = total.shape
    if level >= 8:
        split = total.reshape(rows // (2 * level), 2 * level, width)
        return jnp.broadcast_to(split[:, level - 1 : level, :], split.shape).reshape(rows, width)
    split = total.reshape(rows // 8, 8, width)
    place_in = iota(split.shape, 1)
    row = split[:, level - 1 : level, :]
    for start in range(2 * level, 8, 2 * level):
        later = split[:, start + level - 1 : start + level, :]
        row = jnp.where(place_in >= start, later, row)
    return jnp.broadcast_to(row, split.shape).reshape(rows, width)


def message(state_t, decay_row, doc_row):
    high, mid, low = three_parts(decay_row)
    zeros = jnp.zeros((12, decay_row.shape[1]), F32)
    tail = jnp.concatenate(
        [high.astype(F32), mid.astype(F32), low.astype(F32), doc_row, zeros], axis=0
    )
    return jnp.concatenate([state_t.astype(BF), tail.astype(BF)], axis=0)


def opened(buffer, k, width):
    block = buffer[k].astype(F32)
    state = block[:width]
    decay = block[width : width + 1] + block[width + 1 : width + 2] + block[width + 2 : width + 3]
    return state, decay, block[width + 3 : width + 4]


NAMES = ("q", "k", "v", "g", "dgi", "off", "spk", "doc", "wo", "res", "gain", "shift")
NAMES = NAMES + ("routes", "weights")


def layer_kernel(sizes, *refs):
    hbm = dict(zip(NAMES, refs[: len(NAMES)]))
    wg_hbm, wu_hbm, wd_hbm, out_ref = refs[len(NAMES) : len(NAMES) + 4]
    refs = refs[len(NAMES) + 4 :]
    held = dict(zip(NAMES, refs[: len(NAMES)]))
    (
        isem,
        msg1,
        buf1,
        msg2,
        buf2,
        ql,
        kl,
        oacc,
        pb,
        far,
        near,
        summed,
        send1,
        recv1,
        send2,
        recv2,
        send3,
        recv3,
        wg,
        wu,
        wd,
        tok,
        mix,
        outb,
        inb,
        outq,
        inq,
        xg,
        hid,
        yb,
        ra,
        rs,
        rb,
        backb,
        retb,
        wsem,
        dsend,
        drecv,
        gsend,
        grecv,
        fsend,
        frecv,
        asend,
        arecv,
        nsend,
        nrecv,
        ssend,
        srecv,
        bsend,
        brecv,
        qsend,
        qrecv,
        tsend,
        trecv,
    ) = refs[len(NAMES) :]
    zs, xs, cs, ys = sizes
    z, x, c, y = place(sizes)
    group = xs * cs
    me = x * cs + c
    steps, routed, direct = plan(zs)
    around = [(dx, dc) for dx in range(xs) for dc in range(cs)]
    plus = (z, x, c, lax.rem(y + 1, ys))
    minus = (z, x, c, lax.rem(y + ys - 1, ys))

    def peer(dz, dx, dc):
        return (lax.rem(z + dz, zs), lax.rem(x + dx, xs), lax.rem(c + dc, cs), y)

    partners = [
        peer(dz, dx, dc) for dz in range(zs) for dx, dc in around if dz or dx or dc
    ]
    peers = [peer(0, dx, dc) for dx, dc in around if dx or dc]
    columns = [peer(dz, 0, 0) for dz in range(1, zs)]
    fills = {
        name: pltpu.make_async_copy(hbm[name], held[name], isem.at[n])
        for n, name in enumerate(NAMES)
    }
    for name in ("dgi", "off", "spk", "doc", "k", "v", "q"):
        fills[name].start()
    barrier = greet(partners + [plus, minus])
    for name in ("g", "wo", "routes", "weights", "res", "gain", "shift"):
        fills[name].start()
    loads = [
        pltpu.make_async_copy(src.at[0], dst, wsem.at[n])
        for n, (src, dst) in enumerate(((wg_hbm, wg), (wu_hbm, wu), (wd_hbm, wd)))
    ]
    for load in loads:
        load.start()
    for name in ("dgi", "off", "spk", "doc", "k", "v", "q"):
        fills[name].wait()

    length, hk = held["q"].shape
    hv = held["v"].shape[1]
    heads = held["spk"].shape[0]
    dk = hk // heads
    dv = hv // heads
    lane_head = iota((1, hk), 1) // dk
    vlane_head = iota((1, hv), 1) // dv

    pre = held["dgi"][...].astype(F32) + held["off"][...]
    rate = -(jnp.maximum(-pre, 0.0) + jnp.log1p(jnp.exp(-jnp.abs(pre)))) / decay_norm
    spikes = jnp.concatenate([p.astype(F32) for p in three_parts(held["spk"][...])], axis=0)
    spread_to = iota((3 * heads, hk), 0) % heads == iota((3 * heads, hk), 1) // dk
    rate = rate + dot_tn(spikes.astype(BF), spread_to.astype(BF))
    row_i = iota((length, length), 0)
    col_i = iota((length, length), 1)
    tri = (row_i >= col_i).astype(BF)
    high, mid, low = three_parts(rate)
    total = dot(tri, high) + dot(tri, mid) + dot(tri, low)
    last_total = total[length - 1 : length]

    doc_row = held["doc"][...].astype(F32)
    doc_col = jnp.sum(jnp.where(row_i == col_i, doc_row, 0.0), axis=1, keepdims=True)
    last_doc = doc_col[length - 1 : length]
    last_row = jnp.broadcast_to(last_doc, (1, hk))

    keys = held["k"][...].astype(F32)
    query = held["q"][...].astype(F32) * dk ** (-0.5)
    ends = keys * jnp.exp(jnp.minimum(last_total - total, 0.0))
    ends = jnp.where(doc_col == last_doc, ends, 0.0).astype(BF)
    cross = dot_tn(held["v"][...], ends)
    state_t = jnp.zeros((dv, hk), F32)
    for h in range(heads):
        state_t = state_t + jnp.where(lane_head == h, cross[h * dv : (h + 1) * dv], 0.0)
    first = message(state_t, last_total, last_row)
    msg1[...] = first
    buf1[me] = first
    pl.semaphore_wait(barrier, len(partners) + 2)
    for to in peers:
        remote(msg1, buf1.at[me], send1, recv1, to)

    ql[0] = query.astype(BF)
    kl[0] = keys.astype(BF)
    for n, level in enumerate(LEVELS):
        mark = level_reference(total, level)
        ql[n + 1] = (query * jnp.exp(jnp.minimum(total - mark, 0.0))).astype(BF)
        kl[n + 1] = (keys * jnp.exp(jnp.minimum(mark - total, 0.0))).astype(BF)
    entering = (query * jnp.exp(jnp.minimum(total, 0.0))).astype(BF)
    oacc[...] = jnp.zeros_like(oacc)
    visible = (row_i >= col_i) & (doc_col == doc_row)
    differ = row_i ^ col_i

    def head_work(h, carry):
        keep = lane_head == h
        scores = dot_nt(ql[0], jnp.where(keep, kl[0], jnp.zeros((), BF)))
        for n, level in enumerate(LEVELS):
            at_level = dot_nt(ql[n + 1], jnp.where(keep, kl[n + 1], jnp.zeros((), BF)))
            scores = jnp.where(differ >= level, at_level, scores)
        scores = jnp.where(visible, scores, 0.0).astype(BF)
        oacc[...] += dot(scores, jnp.where(vlane_head == h, held["v"][...], jnp.zeros((), BF)))
        return carry

    lax.fori_loop(0, heads // 2, head_work, 0)

    if group > 1:
        wait_bytes(buf1.at[pl.ds(0, group - 1)], recv1)
    parts = [opened(buf1, j, dv) for j in range(group)]
    group_doc = parts[group - 1][2]
    mine_doc = jnp.full((1, hk), -1.0, F32)
    for j in range(group - 1):
        mine_doc = jnp.where(me == j + 1, parts[j][2], mine_doc)
    group_state = jnp.zeros((dv, hk), F32)
    within = jnp.zeros((dv, hk), F32)
    group_decay = jnp.zeros((1, hk), F32)
    own_decay = jnp.zeros((1, hk), F32)
    for j in range(group - 1, -1, -1):
        state_j, decay_j, doc_j = parts[j]
        share = jnp.where(doc_j == group_doc, jnp.exp(jnp.minimum(group_decay, 0.0)), 0.0)
        group_state = group_state + share * state_j
        group_decay = group_decay + decay_j
        earlier = j < me
        share = jnp.where(doc_j == mine_doc, jnp.exp(jnp.minimum(own_decay, 0.0)), 0.0)
        within = within + jnp.where(earlier, share, 0.0) * state_j
        own_decay = own_decay + jnp.where(earlier, decay_j, 0.0)
    second = message(group_state, group_decay, group_doc)
    msg2[...] = second
    buf2[z] = second
    for to in columns:
        remote(msg2, buf2.at[z], send2, recv2, to)

    lax.fori_loop(heads // 2, heads, head_work, 0)

    fills["routes"].wait()
    fills["weights"].wait()
    rows = length // ys
    half = rows // 2
    model = held["wo"].shape[1]
    cols = model // 4
    spots = group * 16
    keep = group * 4
    halves = keep // 2
    experts = zs * group
    lanes = iota((rows, experts), 1).astype(F32)
    below = (iota((rows, rows), 0) > iota((rows, rows), 1)).astype(BF)
    quarter = (iota((4 * rows, 1), 0) // rows * 4).astype(F32)
    diagonal = iota((4 * rows, 4 * rows), 0) == iota((4 * rows, 4 * rows), 1)
    reach = iota((4 * rows, length), 1) - iota((4 * rows, length), 0) % rows

    def plane_col(name, j, plane):
        row = held[name][j : j + 1, :].astype(F32)
        mask = reach == lax.rem(y + plane, ys) * rows
        return jnp.sum(jnp.where(mask, row, 0.0), axis=1, keepdims=True)

    def plane_slots(plane):
        route_cols = [plane_col("routes", j, plane) for j in range(2)]
        marks = [(route_cols[j][0:rows] == lanes).astype(F32) for j in range(2)]
        before = dot(below, marks[0].astype(BF))
        pos0 = jnp.sum(before * marks[0], axis=1, keepdims=True)
        before = dot(below, marks[1].astype(BF)) + jnp.sum(marks[0], axis=0, keepdims=True)
        pos1 = jnp.sum(before * marks[1], axis=1, keepdims=True)
        slot_cols = []
        slot_rows = []
        for j, pos in ((0, pos0), (1, pos1)):
            one = route_cols[j] * 16 + jnp.concatenate([pos] * 4, axis=0) + quarter
            slot_cols.append(one.astype(jnp.int32))
            as_row = jnp.sum(jnp.where(diagonal, one, 0.0), axis=0, keepdims=True)
            slot_rows.append(as_row.astype(jnp.int32))
        return slot_cols, slot_rows

    planes = (0, ys - 1, 2, 1)
    slots = [plane_slots(planes[0])]
    slot_cols = slots[0][0]
    weight_cols = [plane_col("weights", j, 0) for j in range(2)]

    fills["g"].wait()
    fills["wo"].wait()
    gate = held["g"][...].astype(F32)
    gate = gate / (1.0 + jnp.exp(-gate))

    if zs > 1:
        wait_bytes(buf2.at[pl.ds(0, zs - 1)], recv2)
    parts = [opened(buf2, k, dv) for k in range(zs)]
    for k in range(zs - 1):
        mine_doc = jnp.where((me == 0) & (z == k + 1), parts[k][2], mine_doc)
    for k in range(zs - 1, -1, -1):
        state_k, decay_k, doc_k = parts[k]
        earlier = k < z
        share = jnp.where(doc_k == mine_doc, jnp.exp(jnp.minimum(own_decay, 0.0)), 0.0)
        within = within + jnp.where(earlier, share, 0.0) * state_k
        own_decay = own_decay + jnp.where(earlier, decay_k, 0.0)
    arriving = jnp.concatenate(
        [jnp.where(lane_head == h, within, 0.0).astype(BF) for h in range(heads)], axis=0
    )
    carried = dot_nt(entering, arriving)
    carried = jnp.where(doc_col == mine_doc[:, 0:1], carried, 0.0)
    recurrent = oacc[...] + carried
    same = (iota((hv, hv), 0) // dv == iota((hv, hv), 1) // dv).astype(BF)
    square = recurrent * recurrent
    square_high = square.astype(BF)
    square_low = (square - square_high.astype(F32)).astype(BF)
    mean = (dot(square_high, same) + dot(square_low, same)) / dv
    mixed = (recurrent * lax.rsqrt(mean + eps_rms) * gate).astype(BF)

    tile = model // 4
    for n in range(4):
        pb[:, n * tile : (n + 1) * tile] = dot(
            mixed, held["wo"][:, n * tile : (n + 1) * tile]
        ).astype(BF)

    def mine(offset, start):
        base = lax.rem(y + offset, ys) * rows + start
        return pb.at[pl.ds(pl.multiple_of(base, half), half)]

    remote(mine(2, 0), far.at[0], send3.at[0], recv3.at[0], minus)
    remote(mine(2, half), far.at[1], send3.at[1], recv3.at[1], plus)
    remote(mine(ys - 1, half), near.at[0, 1], send3.at[2], recv3.at[2], minus)
    remote(mine(1, 0), near.at[1, 0], send3.at[3], recv3.at[3], plus)
    slots = slots + [plane_slots(plane) for plane in planes[1:]]
    wait_bytes(far.at[0], recv3.at[0])
    summed[0] = (mine(ys - 1, 0)[...].astype(F32) + far[0].astype(F32)).astype(BF)
    remote(summed.at[0], near.at[0, 0], send3.at[4], recv3.at[4], minus)
    wait_bytes(far.at[1], recv3.at[1])
    summed[1] = (mine(1, half)[...].astype(F32) + far[1].astype(F32)).astype(BF)
    remote(summed.at[1], near.at[1, 1], send3.at[5], recv3.at[5], plus)
    for name in ("res", "gain", "shift"):
        fills[name].wait()
    gain = held["gain"][0:1, :]
    shift = held["shift"][0:1, :]
    wait_bytes(near.at[0, 1], recv3.at[2])
    wait_bytes(near.at[1, 0], recv3.at[3])
    wait_bytes(near.at[0, 0], recv3.at[4])
    wait_bytes(near.at[1, 1], recv3.at[5])
    for s in range(2):
        stream = held["res"][s * half : (s + 1) * half].astype(F32)
        stream = stream + mine(0, s * half)[...].astype(F32)
        stream = stream + near[0, s].astype(F32) + near[1, s].astype(F32)
        center = jnp.mean(stream, axis=-1, keepdims=True)
        moved = stream - center
        spread = jnp.mean(moved * moved, axis=-1, keepdims=True)
        normed = (moved * lax.rsqrt(spread + eps_layer) * gain + shift).astype(BF)
        for n in range(4):
            tok[0, n * rows + s * half : n * rows + (s + 1) * half] = normed[
                :, n * cols : (n + 1) * cols
            ]

    def spot_ids(shape, dim, dz):
        return iota(shape, dim) + lax.rem(z + dz, zs) * spots

    to_rows = iota((spots, spots), 0)
    from_rows = iota((spots, spots), 1)
    arranged = (to_rows % keep // 4) * 16 + (to_rows // keep) * 4 + to_rows % 4
    arrange = (from_rows == arranged).astype(BF)
    arranged = (from_rows % keep // 4) * 16 + (from_rows // keep) * 4 + from_rows % 4
    restore = (to_rows == arranged).astype(BF)

    def picked(p, dz):
        ids = spot_ids((spots, 4 * rows), 0, dz)
        pick = ((ids == slots[p][1][0]) | (ids == slots[p][1][1])).astype(BF)
        return dot(pick, tok[p]).astype(BF)

    def launch(k):
        dz = steps[k]
        if k in routed:
            out, into, send, recv, n = outb.at[k], inb.at[k], dsend, drecv, k
            out[...] = picked(0, dz)
        else:
            n = direct.index(k)
            out, into, send, recv = outq.at[n], inq.at[n], qsend, qrecv
            for p in range(ys):
                out[p] = picked(p, dz)
        for dx, dc in around:
            to = peer(dz, dx, dc)
            from_rows = pl.ds(pl.multiple_of((to[1] * cs + to[2]) * 16, 16), 16)
            to_rows = pl.ds(pl.multiple_of(me * 16, 16), 16)
            if k in routed:
                source, landing = out.at[from_rows], into.at[to_rows]
            else:
                source, landing = out.at[:, from_rows], into.at[:, to_rows]
            if dz or dx or dc:
                remote(source, landing, send.at[n], recv.at[n], to)
            else:
                landing[...] = source[...]

    remote(tok.at[0], tok.at[1], tsend.at[0], trecv.at[0], plus)
    remote(tok.at[0], tok.at[3], tsend.at[1], trecv.at[1], minus)
    for k in routed:
        launch(k)

    def sized(buffer, k, dz):
        count = spots if dz else spots - 16
        return buffer.at[k, pl.ds(0, count)]


    def forward(k):
        wait_bytes(xg.at[k, 1], grecv.at[k, 0])
        remote(
            xg.at[k, 1, pl.ds(0, halves)],
            xg.at[k, 2, pl.ds(0, halves)],
            fsend.at[k, 0],
            frecv.at[k, 0],
            plus,
        )
        wait_bytes(xg.at[k, 3], grecv.at[k, 1])
        remote(
            xg.at[k, 3, pl.ds(halves, halves)],
            xg.at[k, 2, pl.ds(halves, halves)],
            fsend.at[k, 1],
            frecv.at[k, 1],
            minus,
        )

    def tidied(block, k, p):
        flat = dot(arrange, block).astype(BF)
        for n in range(4):
            xg[k, p, :, n * cols : (n + 1) * cols] = flat[n * keep : (n + 1) * keep]

    def tidy(k):
        wait_bytes(inb.at[k], drecv.at[k])
        tidied(inb[k], k, 0)
        remote(xg.at[k, 0], xg.at[k, 1], gsend.at[k, 0], grecv.at[k, 0], plus)
        remote(xg.at[k, 0], xg.at[k, 3], gsend.at[k, 1], grecv.at[k, 1], minus)

    def sized_q(buffer, n):
        count = spots if steps[direct[n]] else spots - 16
        return buffer.at[n, :, pl.ds(0, count)]

    def arrived(k):
        if k in routed:
            wait_bytes(xg.at[k, 2, pl.ds(0, halves)], frecv.at[k, 0])
            wait_bytes(xg.at[k, 2, pl.ds(halves, halves)], frecv.at[k, 1])
            return
        n = direct.index(k)
        if steps[k] or group > 1:
            wait_bytes(sized_q(inq, n), qrecv.at[n])
        for p in range(ys):
            tidied(inq[n, p], k, p)

    units = wg.shape[1]
    tiles = [(n, min(256, units - n)) for n in range(0, units, 256)]

    def feed(k):
        arrived(k)
        if k == 0:
            loads[0].wait()
            loads[1].wait()
        for at, size in tiles:
            block = xg[k].reshape(ys * keep, model)
            gate = dot(block, wg[:, at : at + size])
            up = dot(block, wu[:, at : at + size])
            hid[:, at : at + size] = (gate / (1.0 + jnp.exp(-gate)) * up).astype(BF)
        if k == 0:
            loads[2].wait()
        for at in range(0, model, 256):
            part = dot(hid[...], wd[:, at : at + 256]).astype(BF)
            yb[k, :, :, at : at + 256] = part.reshape(ys, keep, 256)
        low, top = pl.ds(0, halves), pl.ds(halves, halves)
        remote(yb.at[k, 2, low], ra.at[k, 0], asend.at[k, 0], arecv.at[k, 0], minus)
        remote(yb.at[k, 2, top], ra.at[k, 1], asend.at[k, 1], arecv.at[k, 1], plus)
        remote(yb.at[k, 1, top], rb.at[k, 0, top], nsend.at[k, 0], nrecv.at[k, 0], minus)
        remote(yb.at[k, 3, low], rb.at[k, 1, low], nsend.at[k, 1], nrecv.at[k, 1], plus)

    def back(k, dz):
        wait_bytes(ra.at[k, 0], arecv.at[k, 0])
        rs[k, 0] = (yb[k, 1, 0:halves].astype(F32) + ra[k, 0].astype(F32)).astype(BF)
        remote(rs.at[k, 0], rb.at[k, 0, pl.ds(0, halves)], ssend.at[k, 0], srecv.at[k, 0], minus)
        wait_bytes(ra.at[k, 1], arecv.at[k, 1])
        rs[k, 1] = (yb[k, 3, halves:keep].astype(F32) + ra[k, 1].astype(F32)).astype(BF)
        remote(
            rs.at[k, 1], rb.at[k, 1, pl.ds(halves, halves)], ssend.at[k, 1], srecv.at[k, 1], plus
        )

    def finish(k, dz):
        wait_bytes(rb.at[k, 0, pl.ds(halves, halves)], nrecv.at[k, 0])
        wait_bytes(rb.at[k, 1, pl.ds(0, halves)], nrecv.at[k, 1])
        wait_bytes(rb.at[k, 0, pl.ds(0, halves)], srecv.at[k, 0])
        wait_bytes(rb.at[k, 1, pl.ds(halves, halves)], srecv.at[k, 1])
        whole = yb[k, 0].astype(F32) + rb[k, 0].astype(F32) + rb[k, 1].astype(F32)
        whole = whole.astype(BF)
        laid = jnp.concatenate(
            [whole[:, n * cols : (n + 1) * cols] for n in range(4)], axis=0
        )
        backb[k] = dot(restore, laid).astype(BF)
        for dx, dc in around:
            to = peer((zs - dz) % zs, dx, dc)
            target = to[1] * cs + to[2]
            source = backb.at[k, pl.ds(pl.multiple_of(target * 16, 16), 16)]
            landing = retb.at[k, pl.ds(pl.multiple_of(me * 16, 16), 16)]
            if dz or dx or dc:
                remote(source, landing, bsend.at[k], brecv.at[k], to)
            else:
                landing[...] = source[...]

    def gather_in(k, dz):
        if (spots if dz else spots - 16) > 0:
            wait_bytes(sized(retb, k, dz), brecv.at[k])
        ids = spot_ids((4 * rows, spots), 1, dz)
        share = jnp.where(ids == slot_cols[0], weight_cols[0], 0.0)
        share = share + jnp.where(ids == slot_cols[1], weight_cols[1], 0.0)
        high = share.astype(BF)
        low = (share - high.astype(F32)).astype(BF)
        mix[...] += dot(high, retb[k]) + dot(low, retb[k])

    low, top = pl.ds(0, 2 * rows), pl.ds(2 * rows, 2 * rows)
    wait_bytes(tok.at[1], trecv.at[0])
    remote(tok.at[1, low], tok.at[2, low], tsend.at[2], trecv.at[2], plus)
    wait_bytes(tok.at[3], trecv.at[1])
    remote(tok.at[3, top], tok.at[2, top], tsend.at[3], trecv.at[3], minus)
    mix[...] = tok[0].astype(F32)
    lag_m, lag_b, lag_e, lag_c = LAGS
    for t in range(zs + lag_c):
        if t < len(routed):
            tidy(routed[t])
        if t == 0:
            wait_bytes(tok.at[2, low], trecv.at[2])
            wait_bytes(tok.at[2, top], trecv.at[3])
            for k in direct:
                launch(k)
        if 1 <= t < len(routed) + 1:
            forward(routed[t - 1])
        if lag_m <= t < zs + lag_m:
            feed(t - lag_m)
        if lag_b <= t < zs + lag_b:
            back(t - lag_b, steps[t - lag_b])
        if lag_e <= t < zs + lag_e:
            finish(t - lag_e, steps[t - lag_e])
        if lag_c <= t < zs + lag_c:
            gather_in(t - lag_c, steps[t - lag_c])

    pieces = [mix[n * rows : (n + 1) * rows] for n in range(4)]
    center = sum(jnp.sum(piece, axis=1, keepdims=True) for piece in pieces) / model
    pieces = [piece - center for piece in pieces]
    spread = sum(jnp.sum(piece * piece, axis=1, keepdims=True) for piece in pieces) / model
    scale = lax.rsqrt(spread + eps_layer)
    for n in range(4):
        at = slice(n * cols, (n + 1) * cols)
        out_ref[:, at] = (
            pieces[n] * scale * held["gain"][1:2, at] + held["shift"][1:2, at]
        ).astype(BF)

    if group > 1:
        wait_bytes(buf1.at[pl.ds(0, group - 1)], send1)
    if zs > 1:
        wait_bytes(buf2.at[pl.ds(0, zs - 1)], send2)
    for n in range(6):
        wait_bytes(far.at[0], send3.at[n])
    for n in range(2):
        wait_bytes(tok.at[0], tsend.at[n])
        wait_bytes(tok.at[2, low], tsend.at[n + 2])
    for k, dz in enumerate(steps):
        part = xg.at[k, 0, pl.ds(0, halves)]
        if k in routed:
            wait_bytes(outb.at[k], dsend.at[k])
            for n in range(2):
                wait_bytes(xg.at[k, 0], gsend.at[k, n])
                wait_bytes(part, fsend.at[k, n])
        elif dz or group > 1:
            wait_bytes(sized_q(outq, direct.index(k)), qsend.at[direct.index(k)])
        if dz or group > 1:
            wait_bytes(sized(backb, k, dz), bsend.at[k])
        for n in range(2):
            for sem in (asend, nsend, ssend):
                wait_bytes(part, sem.at[k, n])


def layer(sizes, *args):
    named = dict(zip(NAMES, args))
    wg = args[-3]
    zs, xs, cs, ys = sizes
    length, hk = named["q"].shape
    hv = named["v"].shape[1]
    dv = hv // named["spk"].shape[0]
    rows, model = named["res"].shape
    units = wg.shape[2]
    group = xs * cs
    spots, keep, cols = group * 16, group * 4, model // 4
    dma = pltpu.SemaphoreType.DMA
    hbm = pl.BlockSpec(memory_space=pl.ANY)
    half = rows // 2
    wide = len(plan(zs)[2])
    return pl.pallas_call(
        functools.partial(layer_kernel, sizes),
        out_shape=jax.ShapeDtypeStruct((rows, model), BF),
        in_specs=[hbm] * len(args),
        out_specs=pl.BlockSpec(memory_space=pltpu.VMEM),
        scratch_shapes=[pltpu.VMEM(named[name].shape, named[name].dtype) for name in NAMES]
        + [
            dma((len(NAMES),)),
            pltpu.VMEM((dv + 16, hk), BF),
            pltpu.VMEM((group, dv + 16, hk), BF),
            pltpu.VMEM((dv + 16, hk), BF),
            pltpu.VMEM((zs, dv + 16, hk), BF),
            pltpu.VMEM((len(LEVELS) + 1, length, hk), BF),
            pltpu.VMEM((len(LEVELS) + 1, length, hk), BF),
            pltpu.VMEM((length, hv), F32),
            pltpu.VMEM((length, model), BF),
            pltpu.VMEM((2, half, model), BF),
            pltpu.VMEM((2, 2, half, model), BF),
            pltpu.VMEM((2, half, model), BF),
            dma,
            dma,
            dma,
            dma,
            dma((6,)),
            dma((6,)),
            pltpu.VMEM((model, units), BF),
            pltpu.VMEM((model, units), BF),
            pltpu.VMEM((units, model), BF),
            pltpu.VMEM((4, 4 * rows, cols), BF),
            pltpu.VMEM((4 * rows, cols), F32),
            pltpu.VMEM((zs, spots, cols), BF),
            pltpu.VMEM((zs, spots, cols), BF),
            pltpu.VMEM((wide, 4, spots, cols), BF),
            pltpu.VMEM((wide, 4, spots, cols), BF),
            pltpu.VMEM((zs, ys, keep, model), BF),
            pltpu.VMEM((ys * keep, units), BF),
            pltpu.VMEM((zs, ys, keep, model), BF),
            pltpu.VMEM((zs, 2, keep // 2, model), BF),
            pltpu.VMEM((zs, 2, keep // 2, model), BF),
            pltpu.VMEM((zs, 2, keep, model), BF),
            pltpu.VMEM((zs, spots, cols), BF),
            pltpu.VMEM((zs, spots, cols), BF),
            dma((3,)),
            dma((zs,)),
            dma((zs,)),
        ]
        + [dma((zs, 2))] * 10
        + [dma((zs,)), dma((zs,)), dma((wide,)), dma((wide,)), dma((4,)), dma((4,))],
        compiler_params=pltpu.CompilerParams(
            collective_id=0, has_side_effects=True, vmem_limit_bytes=44 * 1024 * 1024
        ),
        name="layer",
    )(*[pltpu.with_memory_space_constraint(a, pltpu.HBM) for a in args])


def on_device(
    sizes,
    residual,
    queries,
    projected_keys,
    values,
    projected_output_gate,
    decay_gate_input,
    decay_gate_offset,
    decay_spikes,
    documents,
    attention_output_weight,
    layer_norm_gains,
    layer_norm_shifts,
    routes,
    chosen_expert_weights,
    expert_gate_weight,
    expert_up_weight,
    expert_down_weight,
):
    return layer(
        sizes,
        queries,
        projected_keys,
        values,
        projected_output_gate,
        decay_gate_input,
        decay_gate_offset.reshape(1, -1),
        decay_spikes.T,
        documents.reshape(1, -1),
        attention_output_weight,
        residual,
        layer_norm_gains,
        layer_norm_shifts,
        routes.T,
        chosen_expert_weights.T,
        expert_gate_weight,
        expert_up_weight,
        expert_down_weight,
    )


def build(torus):
    sizes = tuple(torus.shape[a] for a in SP_TP)
    return jax.shard_map(
        functools.partial(on_device, sizes),
        mesh=torus,
        in_specs=(
            P(SP_TP, None),
            P(SP, "tp"),
            P(SP, "tp"),
            P(SP, "tp"),
            P(SP, "tp"),
            P(SP, "tp"),
            P("tp"),
            P(SP, "tp"),
            P(SP),
            P("tp", None),
            P(),
            P(),
            P(SP, None),
            P(SP, None),
            P(SP, None, "tp"),
            P(SP, None, "tp"),
            P(SP, "tp", None),
        ),
        out_specs=P(SP_TP, None),
        check_vma=False,
    )


def solution(mesh):
    return build(Mesh(mesh.devices.reshape(8, 4, 2, mesh.shape["tp"]), SP_TP))
```

time: 163 us -> 118 us (0.72)
  Pallas kernels: 147 us -> 117 us
  local copies, waits for them, and re-layouts: 15.4 us -> 0.71 us
    pallas_call x2 -> x1, Pallas kernels: 147 us -> 117 us  [layer(): pl.pallas_call(functools.partial(layer_kernel, sizes), out_shape=jax.Shap...]
    unnamed x28 -> x1, local copies, waits for them, and re-layouts: 15.4 us -> 0.71 us
where the time goes in v2:
time: 118 us; the launch traced here: 117 us
  Pallas kernels  117 us (99%)
    pallas_call x1, Pallas kernels, layer(): pl.pallas_call(functools.partial(layer_kernel, sizes), out_shape=jax.Shap...  117 us

profile of v2, /device:TPU:1, one launch (start us, length us, event | category | flops | bytes accessed | tf_op | source)
XLA Modules:
  0.0 117.2 jit_solution(8653372418778308473)
XLA Ops:
  0.0 116.5 %layer.1 = bf16[64,2048]{1,0:T(8,128)(2,1)S(1)} custom-call(bf16[256,128]{1,0:T(8,128)(2,1)} %refs_0_.1, bf16[256,128]{1,0:T(8,128)(2,1)} %refs_1_.1, bf16[256,256]{1,0:T(8,128)(2,1)} %refs_2_.1, bf16[256,256]{1,0:T(8,128)(2,1)} %refs_3_.1, bf16[256,128]{1,0:T(8,128)(2,1)} %refs_4_.1, f32[1,128]{1,0:T(1,128)} %bitcast.9, f32[4,256]{1,0:T(4,128)} %bitcast.5, ...), custom_call_target="tpu_custom_call" | custom-call | tf_op jit(solution)/shard_map/layer/pallas_call | solution.py:662
  116.5 0.7 copy.19

commit v3 on v2

--- a/solution.py
+++ b/solution.py
@@ -13,7 +13,7 @@
 MESH = pl.DeviceIdType.MESH
 F32 = jnp.float32
 BF = jnp.bfloat16
-LAGS = (2, 3, 4, 6)
+LAGS = (2, 3, 4, 8)
 LEVELS = (1, 2, 4, 8, 16, 32, 64, 128)
 
 eps_rms = 1e-06
@@ -56,7 +56,7 @@
 
 def plan(zs):
     direct = (0, 1, zs - 1) if zs >= 4 else (0,)
-    steps = [2, 6, 3, 1, 5, 7, 4, 0] if zs == 8 else offsets(zs)[::-1]
+    steps = [2, 6, 3, 5, 1, 4, 7, 0] if zs == 8 else offsets(zs)[::-1]
     first = [k for k, dz in enumerate(steps) if dz not in direct]
     late = [k for k, dz in enumerate(steps) if dz in direct]
     return steps, first, late

time: 118 us -> 115 us (0.975)
  Pallas kernels: 117 us -> 114 us
    pallas_call x1, Pallas kernels: 117 us -> 114 us  [layer(): pl.pallas_call(functools.partial(layer_kernel, sizes), out_shape=jax.Shap...]
where the time goes in v3:
time: 115 us
  Pallas kernels  114 us (99%)
    pallas_call x1, Pallas kernels, layer(): pl.pallas_call(functools.partial(layer_kernel, sizes), out_shape=jax.Shap...  114 us

profile of v3, /device:TPU:1, one launch (start us, length us, event | category | flops | bytes accessed | tf_op | source)
XLA Modules:
  0.0 114.8 jit_solution(7059226147510426811)
XLA Ops:
  0.0 114.1 %layer.1 = bf16[64,2048]{1,0:T(8,128)(2,1)S(1)} custom-call(bf16[256,128]{1,0:T(8,128)(2,1)} %refs_0_.1, bf16[256,128]{1,0:T(8,128)(2,1)} %refs_1_.1, bf16[256,256]{1,0:T(8,128)(2,1)} %refs_2_.1, bf16[256,256]{1,0:T(8,128)(2,1)} %refs_3_.1, bf16[256,128]{1,0:T(8,128)(2,1)} %refs_4_.1, f32[1,128]{1,0:T(1,128)} %bitcast.9, f32[4,256]{1,0:T(4,128)} %bitcast.5, ...), custom_call_target="tpu_custom_call" | custom-call | tf_op jit(solution)/shard_map/layer/pallas_call | solution.py:662
  114.1 0.7 copy.19
